TPU v7x, 256 devices: a whole 4x4x8 slice. The times are simulated.
256 devices in a mesh: sp: 64 (over z, y, core), tp: 4 (over x).
Axes of the slice: x: 4, y: 4, z: 8, core: 2. Of those that a mesh axis runs over, the one named last changes fastest.
Arguments:
- head_input_values: bfloat16 [24576, 4096], P('sp', 'tp'), may hold values from -6 to 6
- group_input_vectors: bfloat16 [24576, 1024], P('sp', 'tp'), may hold values from -6 to 6
- group_readout_vectors: bfloat16 [24576, 1024], P('sp', 'tp'), may hold values from -6 to 6
- output_gate_values: bfloat16 [24576, 4096], P('sp', 'tp'), may hold values from -6 to 6
- step_size_logits: float32 [24576, 64], P('sp', 'tp'), may hold values from -6 to 6
- extra_log_decay: float32 [24576, 64], P('sp', 'tp'), may hold values from -1.2 to 0
- head_input_filter: bfloat16 [4, 4096], P(None, 'tp'), may hold values from -3 to 3
- input_vector_filter: bfloat16 [4, 1024], P(None, 'tp'), may hold values from -3 to 3
- readout_vector_filter: bfloat16 [4, 1024], P(None, 'tp'), may hold values from -3 to 3
- step_size_bias: float32 [64], P('tp'), may hold values from -0.5 to 0.5
- head_rate_logarithm: float32 [64], P('tp'), may hold values from -20 to -1
- direct_path_weight: float32 [64], P('tp'), may hold values from 0 to 3
- group_norm_scale: bfloat16 [4096], P('tp'), may hold values from 0.099609375 to 1.8984375
- mixer_output_weight: bfloat16 [4096, 2048], P('tp'), may hold values from -0.09375 to 0.09375
- residual: bfloat16 [24576, 2048], P(('sp', 'tp')), may hold values from -6 to 6
- first_norm_scale: float32 [2048], replicated, may hold values from 0.1 to 1.9
- first_norm_bias: float32 [2048], replicated, may hold values from -1.5 to 1.5
- routes: int32 [24576, 2], P(('sp', 'tp')), may hold values from 0 to 63, all different within a row; in each aligned block of 96 rows (0 to 95, 96 to 191, ...) at most 5 rows name the same one
- routing_weight: float32 [24576, 2], P(('sp', 'tp')), may hold values from 0.1 to 0.9
- expert_gate_weight: bfloat16 [64, 2048, 1024], P('sp', None, 'tp'), may hold values from -0.125 to 0.125
- expert_up_weight: bfloat16 [64, 2048, 1024], P('sp', None, 'tp'), may hold values from -0.125 to 0.125
- expert_down_weight: bfloat16 [64, 2048, 1024], P('sp', None, 'tp'), may hold values from -0.1875 to 0.1875
- final_norm_scale: float32 [2048], replicated, may hold values from 0.1 to 1.9
- final_norm_bias: float32 [2048], replicated, may hold values from -1.5 to 1.5
Outputs:
- final: bfloat16 [24576, 2048], P(('sp', 'tp'))
Inputs may be any that keep to these rules, and one draw needn't show every extreme that they name: `routes`: in the rows of one device no expert is named more than 5 times.
All inputs are finite; a program needn't handle non-finite values.
Results may differ from a plain program's by a relative error of at most 0.012.
Values may be sent and summed in bfloat16 or wider, within the bound.
A program may use at most 128 MiB of HBM per device.

v0:
```python
import functools

import jax
import jax.numpy as jnp
from jax import lax
from jax.experimental import pallas as pl
from jax.experimental.pallas import tpu as pltpu
from jax.sharding import PartitionSpec as P

HEAD_DIM = 64
STATE_WIDTH = 128
BLOCK_LENGTH = 128
EPS = 1e-05
ALPHA = 8.0**0.25
LANES = 128
PACK_ROWS = 16

f32 = jnp.float32
bf16 = jnp.bfloat16
VMEM = pl.BlockSpec(memory_space=pltpu.VMEM)


def silu(v):
    return v * (1.0 / (1.0 + jnp.exp(-v)))


def pair_wide(values, pair):
    rows = values.shape[0]
    lane = lax.broadcasted_iota(jnp.int32, (rows, LANES), 1)
    a = jnp.broadcast_to(values[:, 2 * pair : 2 * pair + 1], (rows, LANES))
    b = jnp.broadcast_to(values[:, 2 * pair + 1 : 2 * pair + 2], (rows, LANES))
    return jnp.where(lane < HEAD_DIM, a, b)


def scan_kernel(
    x_ref, b_ref, c_ref, tail_ref, logit_ref, extra_ref, fx_ref, fb_ref, fc_ref,
    bias_ref, rate_ref, direct_ref,
    y_ref, cc_ref, run_ref, pack_ref,
    pad_scr, u_scr, bb_scr, step_scr,
):
    length, width = x_ref.shape
    gw = b_ref.shape[1]
    taps = fx_ref.shape[0]
    heads = logit_ref.shape[1]
    groups = gw // STATE_WIDTH
    per = width // groups
    pairs = per // LANES
    blocks = length // BLOCK_LENGTH
    L = BLOCK_LENGTH
    v = logit_ref[...] + bias_ref[...]
    step = jnp.maximum(v, 0.0) + jnp.log(1.0 + jnp.exp(-jnp.abs(v)))
    step_scr[...] = step
    decay = -step * jnp.exp(rate_ref[...]) + extra_ref[...]
    ti = lax.broadcasted_iota(jnp.int32, (L, L), 0)
    si = lax.broadcasted_iota(jnp.int32, (L, L), 1)
    causal = ti >= si
    tri = causal.astype(f32)
    runs = []
    before = jnp.zeros((1, heads), f32)
    for k in range(blocks):
        r = jnp.dot(tri, decay[k * L : (k + 1) * L], precision=lax.Precision.HIGHEST,
                    preferred_element_type=f32)
        runs.append(r)
        run_ref[k * L : (k + 1) * L, :] = r + before
        before = before + r[L - 1 : L]
    total = before

    def conv(raw_ref, lo, filt_ref, col):
        pad_scr[8 - (taps - 1) : 8, :] = tail_ref[:, lo + col : lo + col + LANES].astype(f32)
        pad_scr[8 : 8 + length, :] = raw_ref[:, col : col + LANES].astype(f32)
        acc = None
        for o in range(taps):
            start = 8 - (taps - 1) + o
            part = pad_scr[start : start + length, :] * filt_ref[o : o + 1, col : col + LANES].astype(f32)
            acc = part if acc is None else acc + part
        return silu(acc)

    for g in range(groups):
        col = g * STATE_WIDTH
        bb_scr[:, col : col + LANES] = conv(b_ref, width, fb_ref, col).astype(bf16)
        cc_ref[:, col : col + LANES] = conv(c_ref, width + gw, fc_ref, col).astype(bf16)
    for p in range(width // LANES):
        col = p * LANES
        xc = conv(x_ref, 0, fx_ref, col)
        y_ref[:, col : col + LANES] = xc * pair_wide(direct_ref[...], p)
        u_scr[:, col : col + LANES] = (xc * pair_wide(step_scr[...], p)).astype(bf16)

    lane = lax.broadcasted_iota(jnp.int32, (L, LANES), 1)
    contract0 = (((0,), (0,)), ((), ()))
    for g in range(groups):
        ncol = g * STATE_WIDTH
        states = [None] * pairs
        for k in range(blocks):
            rows = slice(k * L, (k + 1) * L)
            cb = cc_ref[rows, ncol : ncol + LANES]
            bb = bb_scr[rows, ncol : ncol + LANES]
            bt = bb.T
            prod = lax.dot_general(cb, bb, (((1,), (1,)), ((), ())), preferred_element_type=f32)
            run = runs[k]
            run_t = run.T
            end = run[L - 1 : L]
            enter = jnp.exp(run)
            leave = jnp.exp(end - run)
            whole = jnp.exp(end)
            for p in range(pairs):
                q = g * pairs + p
                cols = slice(q * LANES, (q + 1) * LANES)
                u = u_scr[rows, cols]
                mats = []
                for h in (2 * q, 2 * q + 1):
                    diff = jnp.where(causal, run[:, h : h + 1] - run_t[h : h + 1, :], -1e30)
                    mats.append((prod * jnp.exp(diff)).astype(bf16))
                zero = jnp.zeros_like(u)
                both = jnp.concatenate(
                    [jnp.where(lane < HEAD_DIM, u, zero), jnp.where(lane < HEAD_DIM, zero, u)], axis=0
                )
                out = jnp.dot(jnp.concatenate(mats, axis=1), both, preferred_element_type=f32)
                if k > 0:
                    out = out + pair_wide(enter, q) * jnp.dot(
                        cb, states[p].astype(bf16), preferred_element_type=f32
                    )
                y_ref[rows, cols] = y_ref[rows, cols] + out
                added = jnp.dot(
                    bt, (u.astype(f32) * pair_wide(leave, q)).astype(bf16), preferred_element_type=f32
                )
                states[p] = added if k == 0 else states[p] * pair_wide(whole, q) + added
        for p in range(pairs):
            q = g * pairs + p
            cols = slice(q * LANES, (q + 1) * LANES)
            pack_ref[0:STATE_WIDTH, cols] = states[p].astype(bf16)
            wide = pair_wide(jnp.broadcast_to(total, (PACK_ROWS, heads)), q)
            hi = wide.astype(bf16)
            lo = (wide - hi.astype(f32)).astype(bf16)
            row = lax.broadcasted_iota(jnp.int32, (PACK_ROWS, LANES), 0)
            pack_ref[STATE_WIDTH : STATE_WIDTH + PACK_ROWS, cols] = jnp.where(
                row == 0, hi.astype(f32), lo.astype(f32)
            ).astype(bf16)


def mix_kernel(
    place_ref, y_ref, cc_ref, run_ref, packs_ref, gate_ref, gain_ref, w_ref, *rest
):
    outs, (enter_scr,) = rest[:-1], rest[-1:]
    d = pl.program_id(0)
    width = y_ref.shape[1]
    groups = cc_ref.shape[1] // STATE_WIDTH
    per = width // groups

    @pl.when(d == 0)
    def _():
        place = place_ref[0]
        for p in range(width // LANES):
            cols = slice(p * LANES, (p + 1) * LANES)

            def turn(k, now):
                got = packs_ref[k, :, cols].astype(f32)
                log = got[STATE_WIDTH : STATE_WIDTH + 1] + got[STATE_WIDTH + 1 : STATE_WIDTH + 2]
                return jnp.exp(log) * now + got[0:STATE_WIDTH]

            now = lax.fori_loop(0, place, turn, jnp.zeros((STATE_WIDTH, LANES), f32))
            enter_scr[:, cols] = now.astype(bf16)

    decay = jnp.exp(run_ref[...])
    rows = []
    for g in range(groups):
        cols = slice(g * per, (g + 1) * per)
        cb = cc_ref[:, g * STATE_WIDTH : (g + 1) * STATE_WIDTH]
        read = jnp.dot(cb, enter_scr[:, cols], preferred_element_type=f32)
        wide = jnp.concatenate(
            [pair_wide(decay, g * (per // LANES) + p) for p in range(per // LANES)], axis=1
        )
        gated = (y_ref[:, cols] + read * wide) * silu(gate_ref[:, cols].astype(f32))
        scale = lax.rsqrt(jnp.mean(gated * gated, axis=-1, keepdims=True) + EPS)
        rows.append((gated * scale * gain_ref[:, cols].astype(f32)).astype(bf16))
    out = jnp.dot(jnp.concatenate(rows, axis=1), w_ref[...], preferred_element_type=f32).astype(bf16)
    for k, o_ref in enumerate(outs):

        @pl.when(d == k)
        def _():
            o_ref[...] = out


def norm_rows(values, gain, bias):
    centred = values - jnp.mean(values, axis=-1, keepdims=True)
    spread = jnp.mean(centred * centred, axis=-1, keepdims=True)
    return centred * lax.rsqrt(spread + EPS) * gain + bias


def dispatch_kernel(count, *refs):
    parts = refs[:count]
    res_ref, gain_ref, bias_ref, slots_ref, mid_ref, out_ref = refs[count:]
    mixed = parts[0][...].astype(f32)
    for part in parts[1:]:
        mixed = mixed + part[...].astype(f32)
    middle = norm_rows(ALPHA * res_ref[...].astype(f32) + mixed, gain_ref[...], bias_ref[...]).astype(bf16)
    mid_ref[...] = middle
    n = out_ref.shape[0]
    row = lax.broadcasted_iota(jnp.int32, (n, middle.shape[0]), 0)
    pick = jnp.zeros((n, middle.shape[0]), f32)
    for k in range(slots_ref.shape[0]):
        pick = pick + jnp.where(row == slots_ref[k : k + 1, :], 1.0, 0.0)
    out_ref[...] = jnp.dot(pick.astype(bf16), middle, preferred_element_type=f32).astype(bf16)


def expert_kernel(x_ref, wg_ref, wu_ref, wd_ref, o_ref, acc_ref):
    s = pl.program_id(0)
    x = x_ref[...]
    gate = jnp.dot(x, wg_ref[0, 0], preferred_element_type=f32)
    up = jnp.dot(x, wu_ref[0, 0], preferred_element_type=f32)
    hidden = (silu(gate) * up).astype(bf16)
    part = lax.dot_general(
        hidden, wd_ref[0, 0], (((1,), (1,)), ((), ())), preferred_element_type=f32
    )

    @pl.when(s == 0)
    def _():
        acc_ref[...] = part

    @pl.when(s > 0)
    def _():
        acc_ref[...] += part

    @pl.when(s == pl.num_programs(0) - 1)
    def _():
        o_ref[...] = acc_ref[...].astype(bf16)


def final_kernel(ret_ref, slots_ref, weight_ref, mid_ref, gain_ref, bias_ref, o_ref):
    rows = mid_ref.shape[0]
    n = ret_ref.shape[0]
    col = lax.broadcasted_iota(jnp.int32, (rows, n), 1)
    total = ALPHA * mid_ref[...].astype(f32)
    ffn = None
    for k in range(slots_ref.shape[1]):
        pick = jnp.where(col == slots_ref[:, k : k + 1], 1.0, 0.0).astype(bf16)
        part = jnp.dot(pick, ret_ref[...], preferred_element_type=f32) * weight_ref[:, k : k + 1]
        ffn = part if ffn is None else ffn + part
    o_ref[...] = norm_rows(total + ffn, gain_ref[...], bias_ref[...]).astype(bf16)


def slot_layout(block_routes, capacity, experts):
    flat_routes = block_routes.reshape(-1)
    matches = (flat_routes[:, None] == jnp.arange(experts, dtype=jnp.int32)[None, :]).astype(jnp.int32)
    n = flat_routes.shape[0]
    earlier = jnp.arange(n)[:, None] > jnp.arange(n)[None, :]
    same = flat_routes[:, None] == flat_routes[None, :]
    rank = jnp.sum((earlier & same).astype(jnp.int32), axis=1)
    return flat_routes * capacity + rank


def params(**kw):
    return pltpu.CompilerParams(vmem_limit_bytes=56 * 1024 * 1024, **kw)


def shards(
    head_input_values, group_input_vectors, group_readout_vectors, output_gate_values,
    step_size_logits, extra_log_decay, head_input_filter, input_vector_filter,
    readout_vector_filter, step_size_bias, head_rate_logarithm, direct_path_weight,
    group_norm_scale, mixer_output_weight, residual, first_norm_scale, first_norm_bias,
    routes, routing_weight, expert_gate_weight, expert_up_weight, expert_down_weight,
    final_norm_scale, final_norm_bias,
):
    n_sp, n_tp = lax.axis_size("sp"), lax.axis_size("tp")
    length, width = head_input_values.shape
    gw = group_input_vectors.shape[1]
    heads = step_size_logits.shape[1]
    margin = head_input_filter.shape[0] - 1
    rows_here, model = residual.shape
    top = routes.shape[1]
    local_experts = expert_gate_weight.shape[0]
    experts = local_experts * n_sp
    capacity = max(2, rows_here * top * 5 // (3 * experts))
    slots = experts * capacity

    wg = lax.all_gather(expert_gate_weight, "tp", axis=0)
    wu = lax.all_gather(expert_up_weight, "tp", axis=0)
    wd = lax.all_gather(expert_down_weight, "tp", axis=0)

    tails = jnp.concatenate(
        [a[length - margin :] for a in (head_input_values, group_input_vectors, group_readout_vectors)],
        axis=1,
    )
    tails = lax.ppermute(tails, "sp", [(i, i + 1) for i in range(n_sp - 1)])
    slot_ids = slot_layout(routes, capacity, experts).reshape(rows_here, top)

    y, cc, run, pack = pl.pallas_call(
        scan_kernel,
        out_shape=(
            jax.ShapeDtypeStruct((length, width), f32),
            jax.ShapeDtypeStruct((length, gw), bf16),
            jax.ShapeDtypeStruct((length, heads), f32),
            jax.ShapeDtypeStruct((STATE_WIDTH + PACK_ROWS, width), bf16),
        ),
        in_specs=[VMEM] * 12,
        out_specs=(VMEM,) * 4,
        scratch_shapes=[
            pltpu.VMEM((length + 8, LANES), f32),
            pltpu.VMEM((length, width), bf16),
            pltpu.VMEM((length, gw), bf16),
            pltpu.VMEM((length, heads), f32),
        ],
        compiler_params=params(),
        name="scan_part",
    )(
        head_input_values, group_input_vectors, group_readout_vectors, tails,
        step_size_logits, extra_log_decay, head_input_filter, input_vector_filter,
        readout_vector_filter, step_size_bias.reshape(1, heads),
        head_rate_logarithm.reshape(1, heads), direct_path_weight.reshape(1, heads),
    )
    packs = lax.all_gather(pack, "sp", axis=0)

    where = jnp.stack([lax.axis_index("sp"), lax.axis_index("tp")]).astype(jnp.int32)

    def rotated(d, ref):
        return (lax.rem(ref[1] + d, n_tp), 0)

    def fixed2(d, ref):
        return (0, 0)

    parts = pl.pallas_call(
        mix_kernel,
        grid_spec=pltpu.PrefetchScalarGridSpec(
            num_scalar_prefetch=1,
            grid=(n_tp,),
            in_specs=[
                pl.BlockSpec((rows_here, width), rotated),
                pl.BlockSpec((rows_here, gw), rotated),
                pl.BlockSpec((rows_here, heads), rotated),
                pl.BlockSpec(packs.shape, lambda d, ref: (0, 0, 0)),
                pl.BlockSpec((rows_here, width), rotated),
                pl.BlockSpec((1, width), fixed2),
                pl.BlockSpec((width, model), fixed2),
            ],
            out_specs=[pl.BlockSpec((rows_here, model), fixed2)] * n_tp,
            scratch_shapes=[pltpu.VMEM((STATE_WIDTH, width), bf16)],
        ),
        out_shape=[jax.ShapeDtypeStruct((rows_here, model), bf16)] * n_tp,
        compiler_params=params(dimension_semantics=("arbitrary",)),
        name="mix_part",
    )(where, y, cc, run, packs, output_gate_values, group_norm_scale.reshape(1, width), mixer_output_weight)
    arrived = [parts[0]] + [
        lax.ppermute(parts[d], "tp", [(i, (i + d) % n_tp) for i in range(n_tp)]) for d in range(1, n_tp)
    ]
    middle, outgoing = pl.pallas_call(
        functools.partial(dispatch_kernel, n_tp),
        out_shape=(
            jax.ShapeDtypeStruct((rows_here, model), bf16),
            jax.ShapeDtypeStruct((slots, model), bf16),
        ),
        in_specs=[VMEM] * (n_tp + 4),
        out_specs=(VMEM, VMEM),
        compiler_params=params(),
        name="dispatch_part",
    )(
        *arrived, residual, first_norm_scale.reshape(1, model), first_norm_bias.reshape(1, model),
        slot_ids.T,
    )
    received = lax.all_to_all(
        outgoing.reshape(n_sp, local_experts * capacity, model), "sp", split_axis=0, concat_axis=0, tiled=True
    )
    rows_in = received.reshape(n_sp, local_experts, capacity, model).transpose(1, 0, 2, 3)
    rows_in = rows_in.reshape(local_experts, n_sp * capacity, model)
    hid = expert_gate_weight.shape[2]
    answers = []
    for e in range(local_experts):
        answers.append(
            pl.pallas_call(
                expert_kernel,
                grid=(n_tp,),
                in_specs=[
                    pl.BlockSpec((n_sp * capacity, model), lambda s: (0, 0)),
                    pl.BlockSpec((1, 1, model, hid), lambda s, e=e: (s, e, 0, 0)),
                    pl.BlockSpec((1, 1, model, hid), lambda s, e=e: (s, e, 0, 0)),
                    pl.BlockSpec((1, 1, model, hid), lambda s, e=e: (s, e, 0, 0)),
                ],
                out_specs=pl.BlockSpec((n_sp * capacity, model), lambda s: (0, 0)),
                out_shape=jax.ShapeDtypeStruct((n_sp * capacity, model), bf16),
                scratch_shapes=[pltpu.VMEM((n_sp * capacity, model), f32)],
                compiler_params=params(dimension_semantics=("arbitrary",)),
                name="expert_part",
            )(rows_in[e], wg, wu, wd)
        )
    answers = jnp.stack(answers).reshape(local_experts, n_sp, capacity, model).transpose(1, 0, 2, 3)
    returned = lax.all_to_all(
        answers.reshape(n_sp, local_experts * capacity, model), "sp", split_axis=0, concat_axis=0, tiled=True
    ).reshape(slots, model)
    return pl.pallas_call(
        final_kernel,
        out_shape=jax.ShapeDtypeStruct((rows_here, model), bf16),
        in_specs=[VMEM] * 6,
        out_specs=VMEM,
        compiler_params=params(),
        name="final_part",
    )(
        returned, slot_ids, routing_weight, middle, final_norm_scale.reshape(1, model),
        final_norm_bias.reshape(1, model),
    )


def solution(mesh):
    in_specs = (
        P("sp", "tp"), P("sp", "tp"), P("sp", "tp"), P("sp", "tp"), P("sp", "tp"), P("sp", "tp"),
        P(None, "tp"), P(None, "tp"), P(None, "tp"), P("tp"), P("tp"), P("tp"), P("tp"),
        P("tp", None), P(("sp", "tp"), None), P(), P(), P(("sp", "tp"), None), P(("sp", "tp"), None),
        P("sp", None, "tp"), P("sp", None, "tp"), P("sp", None, "tp"), P(), P(),
    )
    out_specs = P(("sp", "tp"), None)
    return jax.shard_map(shards, mesh=mesh, in_specs=in_specs, out_specs=out_specs, check_vma=False)
```

profile of v0, /device:TPU:1, one launch (start us, length us, event | category | flops | bytes accessed | tf_op | source)
XLA Modules:
  0.0 388.7 jit_solution(12942348916820010152)
XLA Ops:
  6.5 0.7 slice.9
  7.3 0.7 slice.10
  8.0 0.7 slice.11
  8.7 4.6 %collective-permute-start = (bf16[3,1536]{1,0:T(4,128)(2,1)S(1)}, bf16[3,1536]{1,0:T(4,128)(2,1)S(1)}, u32[]{:S(2)}, u32[]{:S(2)}) collective-permute-start(bf16[3,1536]{1,0:T(4,128)(2,1)S(1)} %pad_maximum_fusion), channel_id=1, source_target_pairs={{0,4},{4,8},{8,12},{12,16},{16,20},{20,24},{24,28},{28,32},{32,36}... | collective-permute-start | bytes 27656 | tf_op jit(solution)/shard_map/ppermute | solution.py:283
  13.2 1.6 copy.52.logit_ref
  14.8 1.6 copy.53.extra_ref
  17.0 7.4 %scan_part.1 = (f32[384,1024]{1,0:T(8,128)}, bf16[384,256]{1,0:T(8,128)(2,1)}, f32[384,16]{1,0:T(8,128)}, bf16[144,1024]{1,0:T(8,128)(2,1)}) custom-call(bf16[384,1024]{1,0:T(8,128)(2,1)} %x_ref.1, bf16[384,256]{1,0:T(8,128)(2,1)} %b_ref.1, bf16[384,256]{1,0:T(8,128)(2,1)} %c_ref.1, bf16[3,1536]{1,0:T(4,128)(2,1)} %copy-done.4, f32[384,16]{1,0:T(8,128)} %copy.52.logit_ref, ...), custom_call_target="tpu_custom_call" | custom-call | tf_op jit(solution)/shard_map/scan_part/pallas_call | solution.py:286
  24.4 0.7 all-gather.13.cloned.1.call-update
  25.1 0.7 all-gather.15.cloned.1.call-update
  26.4 0.6 reshape.38.gain_ref
  27.0 0.6 pad_add_fusion.place_ref
  27.7 104.0 %all-gather.9.cloned.1.call-done = bf16[9216,1024]{1,0:T(8,128)(2,1)} async-done(((bf16[144,1024]{1,0:T(8,128)(2,1)}), bf16[9216,1024]{1,0:T(8,128)(2,1)}) %all-gather.9.cloned.1.call-update) | async-done | bytes 18874384 | tf_op jit(solution)/shard_map/all_gather | solution.py:310
  131.7 15.7 %mix_part.1 = (bf16[96,2048]{1,0:T(8,128)(2,1)}, bf16[96,2048]{1,0:T(8,128)(2,1)}, bf16[96,2048]{1,0:T(8,128)(2,1)}, bf16[96,2048]{1,0:T(8,128)(2,1)}) custom-call(s32[2]{0:T(128)} %pad_add_fusion.place_ref, f32[384,1024]{1,0:T(8,128)} %get-tuple-element.15.y_ref, bf16[384,256]{1,0:T(8,128)(2,1)} %get-tuple-element.16.cc_ref, ...), custom_call_target="tpu_custom_call" | custom-call | tf_op jit(solution)/shard_map/mix_part/pallas_call | solution.py:320
  147.4 1.2 collective-permute-start.1
  148.6 2.4 collective-permute-start.2
  151.0 1.2 collective-permute-start.3
  152.9 0.6 copy.56.refs_7_
  153.5 15.0 %collective-permute-done.1.refs_1_ = bf16[96,2048]{1,0:T(8,128)(2,1)S(1)} collective-permute-done((bf16[96,2048]{1,0:T(8,128)(2,1)}, bf16[96,2048]{1,0:T(8,128)(2,1)S(1)}, u32[]{:S(2)}, u32[]{:S(2)}) %collective-permute-start.1) | collective-permute-done | bytes 393248 | tf_op jit(solution)/shard_map/ppermute | solution.py:342
  168.5 17.7 %collective-permute-done.2.refs_2_ = bf16[96,2048]{1,0:T(8,128)(2,1)S(1)} collective-permute-done((bf16[96,2048]{1,0:T(8,128)(2,1)}, bf16[96,2048]{1,0:T(8,128)(2,1)S(1)}, u32[]{:S(2)}, u32[]{:S(2)}) %collective-permute-start.2) | collective-permute-done | bytes 393248 | tf_op jit(solution)/shard_map/ppermute | solution.py:342
  186.1 0.7 copy-done.2
  187.0 3.5 dispatch_part.1
  190.5 2.4 reshape.41
  192.9 63.3 %all_to_all.10 = bf16[64,5,2048]{2,1,0:T(8,128)(2,1)} all-to-all(bf16[64,5,2048]{2,1,0:T(8,128)(2,1)S(1)} %reshape.41), channel_id=1, replica_groups=mesh['sp'=64,'tp'=4] {'sp'}, dimensions={0} | all-to-all | bytes 2621440 | tf_op jit(solution)/shard_map/all_to_all | solution.py:358
  256.3 3.6 squeeze_reshape_transpose_reshape.3.x_ref
  259.9 43.3 %all-gather.11.cloned.1.call-done = bf16[4,2048,256]{2,1,0:T(8,128)(2,1)} async-done(((bf16[1,2048,256]{2,1,0:T(8,128)(2,1)}), bf16[4,2048,256]{2,1,0:T(8,128)(2,1)}) %all-gather.11.cloned.1.call-update) | async-done | bytes 4194320 | tf_op jit(solution)/shard_map/all_gather | solution.py:275
  303.2 10.2 %expert_part.1 = bf16[320,2048]{1,0:T(8,128)(2,1)} custom-call(bf16[320,2048]{1,0:T(8,128)(2,1)} %squeeze_reshape_transpose_reshape.3.x_ref, bf16[4,1,2048,256]{3,2,1,0:T(8,128)(2,1)} %bitcast.17, bf16[4,1,2048,256]{3,2,1,0:T(8,128)(2,1)} %bitcast.15, bf16[4,1,2048,256]{3,2,1,0:T(8,128)(2,1)} %bitcast.16), custom_call_target="tpu_custom_call" | custom-call | tf_op jit(solution)/shard_map/expert_part/pallas_call | solution.py:367
  313.4 3.4 reshape_transpose_reshape_stack.3
  316.8 11.0 %all-to-all-start.1 = ((bf16[64,5,2048]{2,1,0:T(8,128)(2,1)}), bf16[64,5,2048]{2,1,0:T(8,128)(2,1)S(1)}, u32[]{:S(2)}, u32[]{:S(2)}) async-start(bf16[64,5,2048]{2,1,0:T(8,128)(2,1)} %reshape_transpose_reshape_stack.3), calls=%async_computation.1 | async-start | bytes 4194304 | tf_op jit(solution)/shard_map/all_to_all | solution.py:384
  327.8 0.7 copy.57.weight_ref
  328.5 49.0 %all-to-all-done.1 = bf16[64,5,2048]{2,1,0:T(8,128)(2,1)S(1)} async-done(((bf16[64,5,2048]{2,1,0:T(8,128)(2,1)}), bf16[64,5,2048]{2,1,0:T(8,128)(2,1)S(1)}, u32[]{:S(2)}, u32[]{:S(2)}) %all-to-all-start.1) | async-done | bytes 1310752 | tf_op jit(solution)/shard_map/all_to_all | solution.py:384
  377.5 1.4 reshape.42.ret_ref
  378.9 3.3 final_part.1
  (33 shorter events, 2.1 us)
Async XLA Ops:
  6.5 125.1 %all-gather.9.cloned.1.call-start = ((), (), s32[]{:S(2)}) async-start(), calls=%async_computation.2 | async-start | bytes 19169280 | tf_op jit(solution)/shard_map/all_gather | solution.py:310
  8.7 7.7 %collective-permute-start = (bf16[3,1536]{1,0:T(4,128)(2,1)S(1)}, bf16[3,1536]{1,0:T(4,128)(2,1)S(1)}, u32[]{:S(2)}, u32[]{:S(2)}) collective-permute-start(bf16[3,1536]{1,0:T(4,128)(2,1)S(1)} %pad_maximum_fusion), channel_id=1, source_target_pairs={{0,4},{4,8},{8,12},{12,16},{16,20},{20,24},{24,28},{28,32},{32,36}... | collective-permute-start | bytes 27656 | tf_op jit(solution)/shard_map/ppermute | solution.py:283
  16.4 0.6 copy-start.4
  24.3 2.1 copy-start.6
  24.4 235.5 %all-gather.13.cloned.1.call-start = ((), (), s32[]{:S(2)}) async-start(), calls=%async_computation.4 | async-start | bytes 5242880 | tf_op jit(solution)/shard_map/all_gather | solution.py:276
  25.1 234.8 %all-gather.15.cloned.1.call-start = ((), (), s32[]{:S(2)}) async-start(), calls=%async_computation.5 | async-start | bytes 5242880 | tf_op jit(solution)/shard_map/all_gather | solution.py:277
  25.8 277.4 %all-gather.11.cloned.1.call-start = ((), (), s32[]{:S(2)}) async-start(), calls=%async_computation.3 | async-start | bytes 5242880 | tf_op jit(solution)/shard_map/all_gather | solution.py:275
  131.7 20.5 %copy-start.5 = (s32[96,2]{0,1:T(2,128)S(1)}, s32[96,2]{0,1:T(2,128)}, u32[]{:S(2)}) copy-start(s32[96,2]{0,1:T(2,128)} %param.41) | copy-start | bytes 2308
  147.4 21.1 %collective-permute-start.1 = (bf16[96,2048]{1,0:T(8,128)(2,1)}, bf16[96,2048]{1,0:T(8,128)(2,1)S(1)}, u32[]{:S(2)}, u32[]{:S(2)}) collective-permute-start(bf16[96,2048]{1,0:T(8,128)(2,1)} %get-tuple-element.20), channel_id=1, source_target_pairs={{0,1},{1,2},{2,3},{3,0},{4,5},{5,6},{6,7},{7,4},{8,9},{9,10},{10,1... | collective-permute-start | bytes 1179656 | tf_op jit(solution)/shard_map/ppermute | solution.py:342
  148.6 37.6 %collective-permute-start.2 = (bf16[96,2048]{1,0:T(8,128)(2,1)}, bf16[96,2048]{1,0:T(8,128)(2,1)S(1)}, u32[]{:S(2)}, u32[]{:S(2)}) collective-permute-start(bf16[96,2048]{1,0:T(8,128)(2,1)} %get-tuple-element.21), channel_id=1, source_target_pairs={{0,2},{1,3},{2,0},{3,1},{4,6},{5,7},{6,4},{7,5},{8,10},{9,11},{10,... | collective-permute-start | bytes 1179656 | tf_op jit(solution)/shard_map/ppermute | solution.py:342
  151.0 35.1 %collective-permute-start.3 = (bf16[96,2048]{1,0:T(8,128)(2,1)}, bf16[96,2048]{1,0:T(8,128)(2,1)S(1)}, u32[]{:S(2)}, u32[]{:S(2)}) collective-permute-start(bf16[96,2048]{1,0:T(8,128)(2,1)} %get-tuple-element.22), channel_id=1, source_target_pairs={{0,3},{1,0},{2,1},{3,2},{4,7},{5,4},{6,5},{7,6},{8,11},{9,8},{10,9... | collective-permute-start | bytes 1179656 | tf_op jit(solution)/shard_map/ppermute | solution.py:342
  152.9 40.0 %copy-start = (s32[96,2]{1,0:T(8,128)}, s32[96,2]{1,0:T(8,128)S(1)}, u32[]{:S(2)}) copy-start(s32[96,2]{1,0:T(8,128)S(1)} %add.4.slots_ref) | copy-start | bytes 2308
  168.5 17.7 %copy-start.1 = (bf16[96,2048]{1,0:T(8,128)(2,1)}, bf16[96,2048]{1,0:T(8,128)(2,1)S(1)}, u32[]{:S(2)}) copy-start(bf16[96,2048]{1,0:T(8,128)(2,1)S(1)} %collective-permute-done.1.refs_1_) | copy-start | bytes 1179652
  186.1 0.8 copy-start.2
  186.1 0.9 copy-start.3
  316.8 11.0 %copy-start.7 = (f32[96,2]{0,1:T(2,128)S(1)}, f32[96,2]{0,1:T(2,128)}, u32[]{:S(2)}) copy-start(f32[96,2]{0,1:T(2,128)} %param.42) | copy-start | bytes 2308
  316.8 60.7 %all-to-all-start.1 = ((bf16[64,5,2048]{2,1,0:T(8,128)(2,1)}), bf16[64,5,2048]{2,1,0:T(8,128)(2,1)S(1)}, u32[]{:S(2)}, u32[]{:S(2)}) async-start(bf16[64,5,2048]{2,1,0:T(8,128)(2,1)} %reshape_transpose_reshape_stack.3), calls=%async_computation.1 | async-start | bytes 4194304 | tf_op jit(solution)/shard_map/all_to_all | solution.py:384
Sparse Core Ops, SparseCore 0:
  24.5 107.1 all-gather.8
  133.5 63.9 all-gather.12
  199.3 51.0 all-gather.14
  252.1 51.0 all-gather.10
where the time goes:
time: 390 us; the launch traced here: 389 us
  waiting for transfers between devices  231 us (59%)
  blocking collectives  63.3 us (16%)
  Pallas kernels  40.1 us (10%)
  starting transfers between devices  20.5 us (5%)
  local copies, waits for them, and re-layouts  19.9 us (5%)
  between operations  13.2 us (3%)
    all_gather x1, waiting for transfers between devices, shards(): packs = lax.all_gather(pack, 'sp', axis=0)  104 us
    all_to_all x1, blocking collectives, shards(): lax.all_to_all(outgoing.reshape(n_sp, local_experts * capacity, model), '...  63.3 us
    all_to_all x1, waiting for transfers between devices, shards(): lax.all_to_all(answers.reshape(n_sp, local_experts * capacity, model), 's...  49 us
    all_gather x1, waiting for transfers between devices, shards(): wg = lax.all_gather(expert_gate_weight, 'tp', axis=0)  43.3 us
    ppermute x3, waiting for transfers between devices, shards(): lax.ppermute(parts[d], 'tp', [(i, (i + d) % n_tp) for i in range(n_tp)])  32.7 us
    pallas_call x1, Pallas kernels, shards(): pl.pallas_call(mix_kernel, grid_spec=pltpu.PrefetchScalarGridSpec(num_sca...  15.7 us
    all_to_all x1, starting transfers between devices, shards(): lax.all_to_all(answers.reshape(n_sp, local_experts * capacity, model), 's...  11 us
    pallas_call x1, Pallas kernels, shards(): pl.pallas_call(expert_kernel, grid=(n_tp,), in_specs=[pl.BlockSpec((n_sp...  10.2 us
  transfers between devices with their start and end apart: 9, of which 5 were waited for; matrix products, arithmetic and copies ran while one was open for 3% of the time, Pallas kernels for 5%

commit v1 on v0

v1 whole, which is shorter than its diff:
```python
import functools

import jax
import jax.numpy as jnp
from jax import lax
from jax.experimental import pallas as pl
from jax.experimental.pallas import tpu as pltpu
from jax.sharding import PartitionSpec as P

HEAD_DIM = 64
STATE_WIDTH = 128
BLOCK_LENGTH = 128
EPS = 1e-05
ALPHA = 8.0**0.25
LANES = 128
CAP = 5
Y_CORES = 8
PLANES = 8

f32 = jnp.float32
bf16 = jnp.bfloat16
MESH = pl.DeviceIdType.MESH
VMEM = pl.BlockSpec(memory_space=pltpu.VMEM)
SMEM = pl.BlockSpec(memory_space=pltpu.SMEM)
HBM = pl.BlockSpec(memory_space=pltpu.MemorySpace.HBM)


def silu(v):
    return v * (1.0 / (1.0 + jnp.exp(-v)))


def pair_wide(values, pair):
    rows = values.shape[0]
    lane = lax.broadcasted_iota(jnp.int32, (rows, LANES), 1)
    a = jnp.broadcast_to(values[:, 2 * pair : 2 * pair + 1], (rows, LANES))
    b = jnp.broadcast_to(values[:, 2 * pair + 1 : 2 * pair + 2], (rows, LANES))
    return jnp.where(lane < HEAD_DIM, a, b)


def norm_rows(values, gain, bias):
    centred = values - jnp.mean(values, axis=-1, keepdims=True)
    spread = jnp.mean(centred * centred, axis=-1, keepdims=True)
    return centred * lax.rsqrt(spread + EPS) * gain + bias


def plane_of(i):
    return jnp.where(lax.rem(i, 2) == 1, 4 - (i + 1) // 2, 4 + i // 2)


def layer_kernel(
    x_hbm, b_hbm, c_hbm, gate_hbm, logit_ref, extra_ref, fx_ref, fb_ref, fc_ref,
    bias_ref, rate_ref, direct_ref, gain_ref, wout_hbm, res_hbm, g1_ref, b1_ref,
    src_ref, slot_ref, rw_ref, wg_hbm, wu_hbm, wd_hbm, g2_ref, b2_ref,
    o_ref,
    x_scr, b_scr, c_scr, gate_scr, wout_scr, res_scr,
    tailx, tailb, tailc, pad_scr, y_scr, u_scr, bb_scr, cc_scr, run_scr, st_scr, gs_scr,
    logs_out, logs_in, pack, xin, eout, ein,
    part_scr, rs_in, mid3, tmpf, out5, rin, xrow, hid, ansb, fin, wbuf,
    lsem, wlsem, tail_s, tail_r, log_s, log_r, ex_s, ex_r, en_s, en_r, rs_s, rs_r, w_s, w_r, d_s, d_r, f_s, f_r,
):
    n_sp, n_tp = 64, 4
    s = lax.axis_index("sp")
    x = lax.axis_index("tp")
    z = s // Y_CORES
    yc = lax.rem(s, Y_CORES)
    core = lax.rem(s, 2)
    odd = lax.rem(x, 2)
    xp = jnp.where(odd == 1, lax.rem(x + 1, n_tp), lax.rem(x + n_tp - 1, n_tp))
    is_root = core == odd
    length, width = x_scr.shape
    gw = b_scr.shape[1]
    taps = fx_ref.shape[0]
    heads = logit_ref.shape[1]
    groups = gw // STATE_WIDTH
    per = width // groups
    pairs = per // LANES
    panels = width // LANES
    L = BLOCK_LENGTH
    blocks = length // L
    rows_here, model = o_ref.shape
    chunks = model // LANES

    def remote(src, dst, ss, rr, dev):
        return pltpu.make_async_remote_copy(
            src_ref=src, dst_ref=dst, send_sem=ss, recv_sem=rr, device_id=dev, device_id_type=MESH
        )

    here = [
        pltpu.make_async_copy(a, b, lsem.at[i])
        for i, (a, b) in enumerate(
            ((x_hbm, x_scr), (b_hbm, b_scr), (c_hbm, c_scr), (gate_hbm, gate_scr), (wout_hbm, wout_scr), (res_hbm, res_scr))
        )
    ]
    for copy in here:
        copy.start()
    experts_w = (wg_hbm, wu_hbm, wd_hbm)

    @pl.when(is_root)
    def _():
        for m in range(3):
            pltpu.make_async_copy(experts_w[m].at[0], wbuf.at[m, x], wlsem.at[m]).start()

    barrier = pltpu.get_barrier_semaphore()

    def greet(d, carry):
        t = lax.rem(s + d, n_sp)
        pl.semaphore_signal(barrier, inc=1, device_id=(t, x), device_id_type=MESH)

        @pl.when(jnp.logical_or(is_root, lax.rem(t, 2) == 1 - odd))
        def _():
            pl.semaphore_signal(barrier, inc=1, device_id=(t, xp), device_id_type=MESH)

        return carry

    lax.fori_loop(1, n_sp, greet, 0)
    for d in range(1, n_tp):
        pl.semaphore_signal(barrier, inc=1, device_id=(s, lax.rem(x + d, n_tp)), device_id_type=MESH)

    v = logit_ref[...] + bias_ref[...]
    step = jnp.maximum(v, 0.0) + jnp.log(1.0 + jnp.exp(-jnp.abs(v)))
    decay = -step * jnp.exp(rate_ref[...]) + extra_ref[...]
    ti = lax.broadcasted_iota(jnp.int32, (L, L), 0)
    si = lax.broadcasted_iota(jnp.int32, (L, L), 1)
    causal = ti >= si
    tri = causal.astype(f32)
    runs = []
    before = jnp.zeros((1, heads), f32)
    for k in range(blocks):
        r = jnp.dot(tri, decay[k * L : (k + 1) * L], precision=lax.Precision.HIGHEST, preferred_element_type=f32)
        runs.append(r)
        run_scr[k * L : (k + 1) * L, :] = r + before
        before = before + r[L - 1 : L]
    for p in range(panels):
        logs_out[p] = pair_wide(before, p)
    here[3].wait()

    def gate_rows(i, carry):
        rows = pl.ds(pl.multiple_of(i * 32, 32), 32)
        gs_scr[rows, :] = silu(gate_scr[rows, :].astype(f32))
        return carry

    lax.fori_loop(0, length // 32, gate_rows, 0)
    for copy in here[:3]:
        copy.wait()

    pl.semaphore_wait(barrier, n_sp - 1 + n_tp - 1 + jnp.where(is_root, n_sp - 1, n_sp // 2 - 1))

    tails = (
        (x_scr, tailx, 0), (b_scr, tailb, 1), (c_scr, tailc, 2),
    )

    def tail_copy(a, t, i, target):
        return remote(a.at[pl.ds(length - 8, 8)], t, tail_s.at[i], tail_r.at[i], (target, x))

    @pl.when(s < n_sp - 1)
    def _():
        for a, t, i in tails:
            tail_copy(a, t, i, s + 1).start()

    def send_log(d, carry):
        t = lax.rem(s + d, n_sp)
        remote(logs_out.at[lax.rem(t, panels)], logs_in.at[s], log_s, log_r, (t, x)).start()
        return carry

    lax.fori_loop(1, n_sp, send_log, 0)
    logs_in[s] = logs_out[lax.rem(s, panels)]

    def weight_copy(m, k, target):
        return remote(experts_w[m].at[0], wbuf.at[m, x], w_s.at[m, k], w_r.at[m], (s, target))

    @pl.when(is_root)
    def _():
        for m in range(3):
            weight_copy(m, 0, lax.rem(x + 2, n_tp)).start()

    @pl.when(jnp.logical_not(is_root))
    def _():
        for m in range(3):
            weight_copy(m, 0, lax.rem(x + 1, n_tp)).start()
            weight_copy(m, 1, lax.rem(x + 3, n_tp)).start()

    @pl.when(s == 0)
    def _():
        for _, t, _i in tails:
            t[...] = jnp.zeros_like(t)

    @pl.when(s > 0)
    def _():
        for a, t, i in tails:
            tail_copy(a, t, i, s - 1).wait_recv()

    def conv(raw_ref, tail_ref, filt_ref, col):
        pad_scr[0:8, :] = tail_ref[:, col : col + LANES].astype(f32)
        pad_scr[8 : 8 + length, :] = raw_ref[:, col : col + LANES].astype(f32)
        acc = None
        for o in range(taps):
            start = 8 - (taps - 1) + o
            part = pad_scr[start : start + length, :] * filt_ref[o : o + 1, col : col + LANES].astype(f32)
            acc = part if acc is None else acc + part
        return silu(acc)

    for g in range(groups):
        col = g * STATE_WIDTH
        bb_scr[:, col : col + LANES] = conv(b_scr, tailb, fb_ref, col).astype(bf16)
    for g in range(groups):
        ncol = g * STATE_WIDTH
        for p in range(pairs):
            q = g * pairs + p
            cols = slice(q * LANES, (q + 1) * LANES)
            xc = conv(x_scr, tailx, fx_ref, q * LANES)
            y_scr[:, cols] = xc * pair_wide(direct_ref[...], q)
            u_scr[:, cols] = (xc * pair_wide(step, q)).astype(bf16)
            state = None
            for k in range(blocks):
                rows = slice(k * L, (k + 1) * L)
                run = runs[k]
                end = run[L - 1 : L]
                leave = pair_wide(jnp.exp(end - run), q)
                added = lax.dot_general(
                    bb_scr[rows, ncol : ncol + LANES],
                    (u_scr[rows, cols].astype(f32) * leave).astype(bf16),
                    (((0,), (0,)), ((), ())), preferred_element_type=f32,
                )
                state = added if k == 0 else state * pair_wide(jnp.exp(end), q) + added
                if k < blocks - 1:
                    st_scr[k, :, cols] = state.astype(bf16)
            state = state.astype(bf16)
            for r in range(STATE_WIDTH // 16):
                pack[r * panels + q] = state[r * 16 : (r + 1) * 16]

    def send_state(d, carry):
        t = lax.rem(s + d, n_sp)
        remote(pack.at[t], xin.at[s], ex_s, ex_r, (t, x)).start()
        return carry

    lax.fori_loop(1, n_sp, send_state, 0)
    xin[s] = pack[s]

    for g in range(groups):
        col = g * STATE_WIDTH
        cc_scr[:, col : col + LANES] = conv(c_scr, tailc, fc_ref, col).astype(bf16)
    lane = lax.broadcasted_iota(jnp.int32, (L, LANES), 1)
    for g in range(groups):
        ncol = g * STATE_WIDTH
        for k in range(blocks):
            rows = slice(k * L, (k + 1) * L)
            cb = cc_scr[rows, ncol : ncol + LANES]
            bb = bb_scr[rows, ncol : ncol + LANES]
            prod = lax.dot_general(cb, bb, (((1,), (1,)), ((), ())), preferred_element_type=f32)
            run = runs[k]
            run_t = run.T
            enter = jnp.exp(run)
            for p in range(pairs):
                q = g * pairs + p
                cols = slice(q * LANES, (q + 1) * LANES)
                u = u_scr[rows, cols]
                mats = []
                for h in (2 * q, 2 * q + 1):
                    diff = jnp.where(causal, run[:, h : h + 1] - run_t[h : h + 1, :], -1e30)
                    mats.append((prod * jnp.exp(diff)).astype(bf16))
                zero = jnp.zeros_like(u)
                both = jnp.concatenate(
                    [jnp.where(lane < HEAD_DIM, u, zero), jnp.where(lane < HEAD_DIM, zero, u)], axis=0
                )
                out = jnp.dot(jnp.concatenate(mats, axis=1), both, preferred_element_type=f32)
                if k > 0:
                    out = out + pair_wide(enter, q) * jnp.dot(
                        cb, st_scr[k - 1, :, cols], preferred_element_type=f32
                    )
                y_scr[rows, cols] = y_scr[rows, cols] + out

    def got(ref, ss, rr):
        return remote(ref, ref, ss, rr, (lax.rem(s + 1, n_sp), x))

    got(logs_in.at[pl.ds(0, n_sp - 1)], log_s, log_r).wait_recv()
    got(xin.at[pl.ds(0, n_sp - 1)], ex_s, ex_r).wait_recv()
    factors = jnp.exp(logs_in[...].reshape(n_sp, LANES))
    logs_in[...] = factors.reshape(n_sp, 1, LANES)

    def turn(i, now):
        eout[i] = now.astype(bf16)
        return logs_in[i] * now + xin[i].astype(f32)

    lax.fori_loop(0, n_sp, turn, jnp.zeros((16, LANES), f32), unroll=8)

    def send_enter(d, carry):
        t = lax.rem(s + d, n_sp)
        remote(eout.at[t], ein.at[s], en_s, en_r, (t, x)).start()
        return carry

    lax.fori_loop(1, n_sp, send_enter, 0)
    ein[s] = eout[s]
    here[4].wait()
    here[5].wait()
    got(ein.at[pl.ds(0, n_sp - 1)], en_s, en_r).wait_recv()

    enters = [
        jnp.concatenate([ein[r * panels + q] for r in range(STATE_WIDTH // 16)], axis=0) for q in range(panels)
    ]

    def rs_copy(d):
        return remote(part_scr.at[d], rs_in.at[d], rs_s.at[d], rs_r.at[d], (s, lax.rem(x + d, n_tp)))

    def mix_rows(i, carry):
        d = jnp.where(i == 0, 2, jnp.where(i == 1, 1, jnp.where(i == 2, 3, 0)))
        rows = pl.ds(pl.multiple_of(lax.rem(x + d, n_tp) * rows_here, 32), rows_here)
        enter = jnp.exp(run_scr[rows, :])
        normed = []
        for g in range(groups):
            cb = cc_scr[rows, g * STATE_WIDTH : (g + 1) * STATE_WIDTH]
            cols = slice(g * per, (g + 1) * per)
            read = jnp.concatenate(
                [
                    jnp.dot(cb, enters[g * pairs + p], preferred_element_type=f32) * pair_wide(enter, g * pairs + p)
                    for p in range(pairs)
                ],
                axis=1,
            )
            gated = (y_scr[rows, cols] + read) * gs_scr[rows, cols]
            scale = lax.rsqrt(jnp.mean(gated * gated, axis=-1, keepdims=True) + EPS)
            normed.append((gated * scale * gain_ref[:, cols].astype(f32)).astype(bf16))
        part_scr[d] = jnp.dot(
            jnp.concatenate(normed, axis=1), wout_scr[...], preferred_element_type=f32
        ).astype(bf16)

        @pl.when(d != 0)
        def _():
            rs_copy(d).start()

        return carry

    lax.fori_loop(0, n_tp, mix_rows, 0)
    mixed = part_scr[0].astype(f32)
    for d in (1, 3, 2):
        rs_copy(d).wait_recv()
        mixed = mixed + rs_in[d].astype(f32)
    middle = norm_rows(ALPHA * res_scr[...].astype(f32) + mixed, g1_ref[...], b1_ref[...]).astype(bf16).astype(f32)
    for c in range(chunks):
        tmpf[pl.ds(c, rows_here, stride=chunks), :] = middle[:, c * LANES : (c + 1) * LANES]
    mid3[...] = tmpf[0 : rows_here * chunks, :].reshape(rows_here, chunks, LANES).astype(bf16)

    def send_plane(i, carry):
        zt = lax.rem(z + plane_of(i), PLANES)

        def send_one(j, carry):
            t = zt * Y_CORES + lax.rem(yc + j, Y_CORES)
            for k in range(CAP):
                out5[t, k] = mid3[src_ref[t * CAP + k]]
            same = lax.rem(t, 2) == odd
            slot = (i * 2 + jnp.where(same, 0, 1)) * Y_CORES + yc
            mine = jnp.logical_and(t == s, same)

            @pl.when(mine)
            def _():
                rin[slot] = out5[t]

            @pl.when(jnp.logical_not(mine))
            def _():
                remote(out5.at[t], rin.at[slot], d_s, d_r.at[i // 2], (t, jnp.where(same, x, xp))).start()

            return carry

        lax.fori_loop(0, Y_CORES, send_one, 0)
        return carry

    lax.fori_loop(0, PLANES, send_plane, 0)

    quarter = 4 * Y_CORES

    @pl.when(is_root)
    def _():
        for m in range(3):
            pltpu.make_async_copy(experts_w[m].at[0], wbuf.at[m, x], wlsem.at[m]).wait()
            ref = wbuf.at[m, pl.ds(0, n_tp - 1)]
            remote(ref, ref, w_s.at[m, 0], w_r.at[m], (lax.rem(s + 1, n_sp), x)).wait_recv()

        def expert_chunk(ci, carry):
            base = ci * quarter

            @pl.when(ci < 3)
            def _():
                got(rin.at[pl.ds(0, quarter)], d_s, d_r.at[ci]).wait_recv()

            @pl.when(ci == 3)
            def _():
                got(rin.at[pl.ds(0, quarter - 1)], d_s, d_r.at[ci]).wait_recv()

            n = quarter * CAP
            tmpf[...] = rin[pl.ds(base, quarter)].astype(f32).reshape(n * chunks, LANES)
            for c in range(chunks):
                xrow[:, c * LANES : (c + 1) * LANES] = tmpf[pl.ds(c, n, stride=chunks), :].astype(bf16)
            for t in range(n_tp):
                gate = jnp.dot(xrow[...], wbuf[0, t], preferred_element_type=f32)
                up = jnp.dot(xrow[...], wbuf[1, t], preferred_element_type=f32)
                hid[t] = (silu(gate) * up).astype(bf16)
            for o in range(chunks // 2):
                ans = None
                for t in range(n_tp):
                    part = lax.dot_general(
                        hid[t], wbuf[2, t, 2 * o * LANES : 2 * (o + 1) * LANES, :],
                        (((1,), (1,)), ((), ())), preferred_element_type=f32,
                    )
                    ans = part if ans is None else ans + part
                tmpf[pl.ds(2 * o, n, stride=chunks), :] = ans[:, :LANES]
                tmpf[pl.ds(2 * o + 1, n, stride=chunks), :] = ans[:, LANES:]
            ansb[pl.ds(base, quarter)] = tmpf[...].reshape(quarter, CAP, chunks, LANES).astype(bf16)

            def send_back(m, carry):
                slot = base + m
                i = slot // 16
                same = lax.rem(slot // 8, 2) == 0
                t = lax.rem(z + PLANES - plane_of(i), PLANES) * Y_CORES + lax.rem(slot, 8)
                mine = jnp.logical_and(t == s, same)

                @pl.when(mine)
                def _():
                    fin[s] = ansb[slot]

                @pl.when(jnp.logical_not(mine))
                def _():
                    remote(ansb.at[slot], fin.at[s], f_s, f_r, (t, jnp.where(same, x, xp))).start()

                return carry

            lax.fori_loop(0, quarter, send_back, 0)
            return carry

        lax.fori_loop(0, 4, expert_chunk, 0)
        got(fin.at[pl.ds(0, n_sp - 1)], f_s, f_r).wait_recv()

    @pl.when(jnp.logical_not(is_root))
    def _():
        got(fin.at[pl.ds(0, n_sp)], f_s, f_r).wait_recv()

    def combine(r, carry):
        total = ALPHA * mid3[r].astype(f32)
        ffn = None
        for k in range(2):
            slot = slot_ref[2 * r + k]
            part = fin[slot // CAP, lax.rem(slot, CAP)].astype(f32) * rw_ref[2 * r + k]
            ffn = part if ffn is None else ffn + part
        tmpf[pl.ds(pl.multiple_of(r * chunks, chunks), chunks), :] = total + ffn
        return carry

    lax.fori_loop(0, rows_here, combine, 0, unroll=4)
    total = jnp.concatenate([tmpf[pl.ds(c, rows_here, stride=chunks), :] for c in range(chunks)], axis=1)
    o_ref[...] = norm_rows(total, g2_ref[...], b2_ref[...]).astype(bf16)

    @pl.when(s < n_sp - 1)
    def _():
        for a, t, i in tails:
            tail_copy(a, t, i, s + 1).wait_send()

    got(logs_in.at[pl.ds(0, n_sp - 1)], log_s, log_r).wait_send()
    got(xin.at[pl.ds(0, n_sp - 1)], ex_s, ex_r).wait_send()
    got(ein.at[pl.ds(0, n_sp - 1)], en_s, en_r).wait_send()
    for d in range(1, n_tp):
        rs_copy(d).wait_send()

    @pl.when(is_root)
    def _():
        for m in range(3):
            weight_copy(m, 0, lax.rem(x + 2, n_tp)).wait_send()
        got(out5.at[pl.ds(0, n_sp - 1)], d_s, d_r.at[0]).wait_send()
        got(ansb.at[pl.ds(0, 2 * n_sp - 1)], f_s, f_r).wait_send()

    @pl.when(jnp.logical_not(is_root))
    def _():
        for m in range(3):
            weight_copy(m, 0, lax.rem(x + 1, n_tp)).wait_send()
            weight_copy(m, 1, lax.rem(x + 3, n_tp)).wait_send()
        got(out5.at[pl.ds(0, n_sp)], d_s, d_r.at[0]).wait_send()


def slot_layout(block_routes, capacity, experts):
    flat_routes = block_routes.reshape(-1)
    n = flat_routes.shape[0]
    earlier = jnp.arange(n)[:, None] > jnp.arange(n)[None, :]
    same = flat_routes[:, None] == flat_routes[None, :]
    rank = jnp.sum((earlier & same).astype(jnp.int32), axis=1)
    slots = flat_routes * capacity + rank
    hit = slots[:, None] == jnp.arange(experts * capacity, dtype=jnp.int32)[None, :]
    source = jnp.sum(jnp.where(hit, (jnp.arange(n, dtype=jnp.int32) // block_routes.shape[1])[:, None], 0), axis=0)
    return slots, source


def shards(
    head_input_values, group_input_vectors, group_readout_vectors, output_gate_values,
    step_size_logits, extra_log_decay, head_input_filter, input_vector_filter,
    readout_vector_filter, step_size_bias, head_rate_logarithm, direct_path_weight,
    group_norm_scale, mixer_output_weight, residual, first_norm_scale, first_norm_bias,
    routes, routing_weight, expert_gate_weight, expert_up_weight, expert_down_weight,
    final_norm_scale, final_norm_bias,
):
    n_sp, n_tp = lax.axis_size("sp"), lax.axis_size("tp")
    length, width = head_input_values.shape
    gw = group_input_vectors.shape[1]
    heads = step_size_logits.shape[1]
    rows_here, model = residual.shape
    hidden = expert_gate_weight.shape[2]
    chunks = model // LANES
    panels = width // LANES
    slots, source = slot_layout(routes, CAP, n_sp)
    dma = pltpu.SemaphoreType.DMA
    quarter_rows = 4 * Y_CORES * CAP
    return pl.pallas_call(
        layer_kernel,
        out_shape=jax.ShapeDtypeStruct((rows_here, model), bf16),
        in_specs=[HBM] * 4 + [VMEM] * 9 + [HBM] * 2 + [VMEM] * 2 + [SMEM] * 3 + [HBM] * 3 + [VMEM] * 2,
        out_specs=VMEM,
        scratch_shapes=[
            pltpu.VMEM((length, width), bf16),
            pltpu.VMEM((length, gw), bf16),
            pltpu.VMEM((length, gw), bf16),
            pltpu.VMEM((length, width), bf16),
            pltpu.VMEM((width, model), bf16),
            pltpu.VMEM((rows_here, model), bf16),
            pltpu.VMEM((8, width), bf16),
            pltpu.VMEM((8, gw), bf16),
            pltpu.VMEM((8, gw), bf16),
            pltpu.VMEM((length + 8, LANES), f32),
            pltpu.VMEM((length, width), f32),
            pltpu.VMEM((length, width), bf16),
            pltpu.VMEM((length, gw), bf16),
            pltpu.VMEM((length, gw), bf16),
            pltpu.VMEM((length, heads), f32),
            pltpu.VMEM((2, STATE_WIDTH, width), bf16),
            pltpu.VMEM((length, width), f32),
            pltpu.VMEM((panels, 1, LANES), f32),
            pltpu.VMEM((n_sp, 1, LANES), f32),
            pltpu.VMEM((n_sp, 16, LANES), bf16),
            pltpu.VMEM((n_sp, 16, LANES), bf16),
            pltpu.VMEM((n_sp, 16, LANES), bf16),
            pltpu.VMEM((n_sp, 16, LANES), bf16),
            pltpu.VMEM((n_tp, rows_here, model), bf16),
            pltpu.VMEM((n_tp, rows_here, model), bf16),
            pltpu.VMEM((rows_here, chunks, LANES), bf16),
            pltpu.VMEM((quarter_rows * chunks, LANES), f32),
            pltpu.VMEM((n_sp, CAP, chunks, LANES), bf16),
            pltpu.VMEM((2 * n_sp, CAP, chunks, LANES), bf16),
            pltpu.VMEM((quarter_rows, model), bf16),
            pltpu.VMEM((n_tp, quarter_rows, hidden), bf16),
            pltpu.VMEM((2 * n_sp, CAP, chunks, LANES), bf16),
            pltpu.VMEM((n_sp, CAP, chunks, LANES), bf16),
            pltpu.VMEM((3, n_tp, model, hidden), bf16),
            dma((6,)), dma((3,)), dma((3,)), dma((3,)), dma, dma, dma, dma, dma, dma,
            dma((n_tp,)), dma((n_tp,)), dma((3, 2)), dma((3,)), dma, dma((4,)), dma, dma,
        ],
        compiler_params=pltpu.CompilerParams(
            collective_id=0, has_side_effects=True, vmem_limit_bytes=60 * 1024 * 1024
        ),
        name="layer",
    )(
        head_input_values, group_input_vectors, group_readout_vectors, output_gate_values,
        step_size_logits, extra_log_decay, head_input_filter, input_vector_filter, readout_vector_filter,
        step_size_bias.reshape(1, heads), head_rate_logarithm.reshape(1, heads), direct_path_weight.reshape(1, heads),
        group_norm_scale.reshape(1, width), mixer_output_weight, residual,
        first_norm_scale.reshape(1, model), first_norm_bias.reshape(1, model),
        source, slots, routing_weight.reshape(-1),
        expert_gate_weight, expert_up_weight, expert_down_weight,
        final_norm_scale.reshape(1, model), final_norm_bias.reshape(1, model),
    )


def solution(mesh):
    in_specs = (
        P("sp", "tp"), P("sp", "tp"), P("sp", "tp"), P("sp", "tp"), P("sp", "tp"), P("sp", "tp"),
        P(None, "tp"), P(None, "tp"), P(None, "tp"), P("tp"), P("tp"), P("tp"), P("tp"),
        P("tp", None), P(("sp", "tp"), None), P(), P(), P(("sp", "tp"), None), P(("sp", "tp"), None),
        P("sp", None, "tp"), P("sp", None, "tp"), P("sp", None, "tp"), P(), P(),
    )
    out_specs = P(("sp", "tp"), None)
    return jax.shard_map(shards, mesh=mesh, in_specs=in_specs, out_specs=out_specs, check_vma=False)
```

time: 390 us -> 176 us (0.45)
  waiting for transfers between devices: 231 us -> 0 us
  Pallas kernels: 40.1 us -> 165 us
  blocking collectives: 63.3 us -> 0 us
  starting transfers between devices: 20.5 us -> 0 us
  between operations: 13.2 us -> 0.03 us
  local copies, waits for them, and re-layouts: 19.9 us -> 8.55 us
    all_gather x4 -> x0, waiting for transfers between devices: 147 us -> none  [the longest x1 104 us: shards(): packs = lax.all_gather(pack, 'sp', axis=0)]
    pallas_call x5 -> x1, Pallas kernels: 40.1 us -> 165 us  [shards(): pl.pallas_call(layer_kernel, out_shape=jax.ShapeDtypeStruct((rows_here, m...]
    all_to_all x1 -> x0, blocking collectives: 63.3 us -> none  [shards(): lax.all_to_all(outgoing.reshape(n_sp, local_experts * capacity, model), '...]
    all_to_all x1 -> x0, waiting for transfers between devices: 49 us -> none  [shards(): lax.all_to_all(answers.reshape(n_sp, local_experts * capacity, model), 's...]
    ppermute x4 -> x0, waiting for transfers between devices: 32.7 us -> none  [the longest x3 32.7 us: shards(): lax.ppermute(parts[d], 'tp', [(i, (i + d) % n_tp) for i in range(n_tp)])]
    all_to_all x1 -> x0, starting transfers between devices: 11 us -> none  [shards(): lax.all_to_all(answers.reshape(n_sp, local_experts * capacity, model), 's...]
    ppermute x4 -> x0, starting transfers between devices: 9.35 us -> none  [the longest x3 4.77 us: shards(): lax.ppermute(parts[d], 'tp', [(i, (i + d) % n_tp) for i in range(n_tp)])]
    another operation x2 -> x0, local copies, waits for them, and re-layouts: 7.02 us -> none  [the longest x1 3.64 us: shards(): rows_in[e]]
  transfers between devices with their start and end apart: 9 -> 0, of which waited for: 5 -> 0; matrix products, arithmetic and copies ran while one was open for 3% -> 0% of each run, Pallas kernels for 5% -> 0%
where the time goes in v1:
time: 176 us; the launch traced here: 175 us
  Pallas kernels  165 us (94%)
  local copies, waits for them, and re-layouts  8.55 us (5%)
    pallas_call x1, Pallas kernels, shards(): pl.pallas_call(layer_kernel, out_shape=jax.ShapeDtypeStruct((rows_here, m...  165 us
    unnamed x7, local copies, waits for them, and re-layouts  6.41 us

profile of v1, /device:TPU:1, one launch (start us, length us, event | category | flops | bytes accessed | tf_op | source)
XLA Modules:
  0.0 174.8 jit_solution(10298382209174660695)
XLA Ops:
  0.0 1.3 reshape.56.gain_ref
  1.3 0.8 copy.31
  2.1 0.1 reshape.59
  2.2 0.2 convert_reduce_fusion
  2.4 0.0 copy-start
  2.4 0.7 select_reduce_fusion.src_ref
  3.1 0.8 copy.32
  3.9 0.7 reshape.60.rw_ref
  4.6 1.5 copy.33.logit_ref
  6.2 1.5 copy.34.extra_ref
  7.7 0.0 copy-done
  7.7 165.3 %layer.1 = bf16[96,2048]{1,0:T(8,128)(2,1)} custom-call(bf16[384,1024]{1,0:T(8,128)(2,1)} %x_hbm.1, bf16[384,256]{1,0:T(8,128)(2,1)} %b_hbm.1, bf16[384,256]{1,0:T(8,128)(2,1)} %c_hbm.1, bf16[384,1024]{1,0:T(8,128)(2,1)} %gate_hbm.1, f32[384,16]{1,0:T(8,128)} %copy.33.logit_ref, f32[384,16]{1,0:T(8,128)} %copy.34.extra_ref, bf16[4,1024]{1,0:T(4,128)(2,1)} %fx_ref.1, ...), custom_call_target="tpu_custom_call" | custom-call | tf_op jit(solution)/shard_map/layer/pallas_call | solution.py:506
  173.0 1.8 %copy.36 = bf16[96,2048]{1,0:T(8,128)(2,1)} copy(bf16[96,2048]{1,0:T(8,128)(2,1)} %layer.1) | data formatting | bytes 786432
  (1 shorter events, 0.0 us)
Async XLA Ops:
  2.4 5.3 %copy-start = (s32[192]{0:T(256)}, s32[192]{0:T(256)S(1)}, u32[]{:S(2)}) copy-start(s32[192]{0:T(256)S(1)} %get-tuple-element.6.slot_ref) | copy-start | bytes 2308

commit v2 on v1

--- a/solution.py
+++ b/solution.py
@@ -14,6 +14,7 @@
 ALPHA = 8.0**0.25
 LANES = 128
 CAP = 5
+N_EXPERTS = 64
 Y_CORES = 8
 PLANES = 8
 
@@ -43,8 +44,7 @@
     return centred * lax.rsqrt(spread + EPS) * gain + bias
 
 
-def plane_of(i):
-    return jnp.where(lax.rem(i, 2) == 1, 4 - (i + 1) // 2, 4 + i // 2)
+SHIFTS = (3, 5, 4, 0, 2, 6, 1, 7)
 
 
 def layer_kernel(
@@ -55,7 +55,7 @@
     x_scr, b_scr, c_scr, gate_scr, wout_scr, res_scr,
     tailx, tailb, tailc, pad_scr, y_scr, u_scr, bb_scr, cc_scr, run_scr, st_scr, gs_scr,
     logs_out, logs_in, pack, xin, eout, ein,
-    part_scr, rs_in, mid3, tmpf, out5, rin, xrow, hid, ansb, fin, wbuf,
+    part_scr, relay, rs_in, mid3, tmpf, out5, rin, xrow, gated_scr, hid, ansb, fin, stage, wbuf,
     lsem, wlsem, tail_s, tail_r, log_s, log_r, ex_s, ex_r, en_s, en_r, rs_s, rs_r, w_s, w_r, d_s, d_r, f_s, f_r,
 ):
     n_sp, n_tp = 64, 4
@@ -65,12 +65,17 @@
     yc = lax.rem(s, Y_CORES)
     core = lax.rem(s, 2)
     odd = lax.rem(x, 2)
-    xp = jnp.where(odd == 1, lax.rem(x + 1, n_tp), lax.rem(x + n_tp - 1, n_tp))
+    right, left = lax.rem(x + 1, n_tp), lax.rem(x + n_tp - 1, n_tp)
+
+    def beyond(plane):
+        return jnp.where(lax.rem(plane, 2) == 0, right, left)
+
+    xp = jnp.where(lax.rem(z, 2) == 0, left, right)
     is_root = core == odd
     length, width = x_scr.shape
     gw = b_scr.shape[1]
     taps = fx_ref.shape[0]
-    heads = logit_ref.shape[1]
+    heads = logit_ref.shape[0]
     groups = gw // STATE_WIDTH
     per = width // groups
     pairs = per // LANES
@@ -94,39 +99,83 @@
     for copy in here:
         copy.start()
     experts_w = (wg_hbm, wu_hbm, wd_hbm)
+    half = model // 2
+
+    def own_weight(m):
+        return pltpu.make_async_copy(experts_w[m].at[0], wbuf.at[m, x], wlsem.at[m])
 
     @pl.when(is_root)
     def _():
         for m in range(3):
-            pltpu.make_async_copy(experts_w[m].at[0], wbuf.at[m, x], wlsem.at[m]).start()
+            own_weight(m).start()
+
+    piece = model // 4
+    pieces = [(0, 0, model, 0)] + [(1, q * piece, piece, 1) for q in range(4)] + [
+        (2, q * piece, piece, 2 + q) for q in range(4)
+    ]
+
+    def send_weight(k):
+        m, first, count, sem = pieces[k]
+        rows = pl.ds(first, count)
+
+        def send(target):
+            remote(experts_w[m].at[0, rows], wbuf.at[m, x, rows], w_s.at[k], w_r.at[sem], (s, target)).start()
+
+        @pl.when(is_root)
+        def _():
+            send(lax.rem(x + 2, n_tp))
+
+        @pl.when(jnp.logical_not(is_root))
+        def _():
+            send(lax.rem(x + 1, n_tp))
+            send(lax.rem(x + 3, n_tp))
+
+    def sent_weight(k, root):
+        m, first, count, sem = pieces[k]
+        ref = wbuf.at[m, 0, pl.ds(first, count)] if root else wbuf.at[m, pl.ds(0, 2), pl.ds(first, count)]
+        remote(ref, ref, w_s.at[k], w_r.at[sem], (lax.rem(s + 1, n_sp), x)).wait_send()
 
     barrier = pltpu.get_barrier_semaphore()
 
     def greet(d, carry):
         t = lax.rem(s + d, n_sp)
         pl.semaphore_signal(barrier, inc=1, device_id=(t, x), device_id_type=MESH)
-
-        @pl.when(jnp.logical_or(is_root, lax.rem(t, 2) == 1 - odd))
-        def _():
+        return carry
+
+    lax.fori_loop(1, n_sp, greet, 0)
+
+    def greet_experts(k, carry):
+        t = 2 * k + 1 - odd
+        pl.semaphore_signal(barrier, inc=1, device_id=(t, beyond(t // Y_CORES)), device_id_type=MESH)
+        return carry
+
+    lax.fori_loop(0, n_sp // 2, greet_experts, 0)
+
+    @pl.when(is_root)
+    def _():
+        def greet_senders(t, carry):
             pl.semaphore_signal(barrier, inc=1, device_id=(t, xp), device_id_type=MESH)
-
-        return carry
-
-    lax.fori_loop(1, n_sp, greet, 0)
+            return carry
+
+        lax.fori_loop(0, n_sp, greet_senders, 0)
+
     for d in range(1, n_tp):
         pl.semaphore_signal(barrier, inc=1, device_id=(s, lax.rem(x + d, n_tp)), device_id_type=MESH)
 
-    v = logit_ref[...] + bias_ref[...]
-    step = jnp.maximum(v, 0.0) + jnp.log(1.0 + jnp.exp(-jnp.abs(v)))
-    decay = -step * jnp.exp(rate_ref[...]) + extra_ref[...]
+    v = logit_ref[...] + bias_ref[...].T
+    step_t = jnp.maximum(v, 0.0) + jnp.log(1.0 + jnp.exp(-jnp.abs(v)))
+    decay_t = -step_t * jnp.exp(rate_ref[...].T) + extra_ref[...]
+    step = step_t.T
     ti = lax.broadcasted_iota(jnp.int32, (L, L), 0)
     si = lax.broadcasted_iota(jnp.int32, (L, L), 1)
     causal = ti >= si
-    tri = causal.astype(f32)
-    runs = []
+    tri = (ti <= si).astype(f32)
+    runs, runs_t = [], []
     before = jnp.zeros((1, heads), f32)
     for k in range(blocks):
-        r = jnp.dot(tri, decay[k * L : (k + 1) * L], precision=lax.Precision.HIGHEST, preferred_element_type=f32)
+        r_t = jnp.dot(decay_t[:, k * L : (k + 1) * L], tri, precision=lax.Precision.HIGHEST, preferred_element_type=f32)
+        r = r_t.T
+        runs_t.append(r_t)
         runs.append(r)
         run_scr[k * L : (k + 1) * L, :] = r + before
         before = before + r[L - 1 : L]
@@ -143,7 +192,7 @@
     for copy in here[:3]:
         copy.wait()
 
-    pl.semaphore_wait(barrier, n_sp - 1 + n_tp - 1 + jnp.where(is_root, n_sp - 1, n_sp // 2 - 1))
+    pl.semaphore_wait(barrier, n_sp - 1 + n_tp - 1 + n_sp // 2 + jnp.where(is_root, n_sp, 0))
 
     tails = (
         (x_scr, tailx, 0), (b_scr, tailb, 1), (c_scr, tailc, 2),
@@ -165,19 +214,8 @@
     lax.fori_loop(1, n_sp, send_log, 0)
     logs_in[s] = logs_out[lax.rem(s, panels)]
 
-    def weight_copy(m, k, target):
-        return remote(experts_w[m].at[0], wbuf.at[m, x], w_s.at[m, k], w_r.at[m], (s, target))
-
-    @pl.when(is_root)
-    def _():
-        for m in range(3):
-            weight_copy(m, 0, lax.rem(x + 2, n_tp)).start()
-
-    @pl.when(jnp.logical_not(is_root))
-    def _():
-        for m in range(3):
-            weight_copy(m, 0, lax.rem(x + 1, n_tp)).start()
-            weight_copy(m, 1, lax.rem(x + 3, n_tp)).start()
+    send_weight(0)
+    send_weight(1)
 
     @pl.when(s == 0)
     def _():
@@ -248,7 +286,7 @@
             bb = bb_scr[rows, ncol : ncol + LANES]
             prod = lax.dot_general(cb, bb, (((1,), (1,)), ((), ())), preferred_element_type=f32)
             run = runs[k]
-            run_t = run.T
+            run_t = runs_t[k]
             enter = jnp.exp(run)
             for p in range(pairs):
                 q = g * pairs + p
@@ -298,8 +336,13 @@
         jnp.concatenate([ein[r * panels + q] for r in range(STATE_WIDTH // 16)], axis=0) for q in range(panels)
     ]
 
-    def rs_copy(d):
-        return remote(part_scr.at[d], rs_in.at[d], rs_s.at[d], rs_r.at[d], (s, lax.rem(x + d, n_tp)))
+    def rs_copy(k):
+        src, dst, target = (
+            (part_scr.at[2, 0], relay.at[0], right), (part_scr.at[2, 1], relay.at[1], left),
+            (part_scr.at[1, 0], rs_in.at[0, 0], right), (part_scr.at[1, 1], rs_in.at[0, 1], right),
+            (part_scr.at[3, 0], rs_in.at[1, 0], left), (part_scr.at[3, 1], rs_in.at[1, 1], left),
+        )[k]
+        return remote(src, dst, rs_s.at[k], rs_r.at[k], (s, target))
 
     def mix_rows(i, carry):
         d = jnp.where(i == 0, 2, jnp.where(i == 1, 1, jnp.where(i == 2, 3, 0)))
@@ -318,131 +361,217 @@
             )
             gated = (y_scr[rows, cols] + read) * gs_scr[rows, cols]
             scale = lax.rsqrt(jnp.mean(gated * gated, axis=-1, keepdims=True) + EPS)
-            normed.append((gated * scale * gain_ref[:, cols].astype(f32)).astype(bf16))
-        part_scr[d] = jnp.dot(
-            jnp.concatenate(normed, axis=1), wout_scr[...], preferred_element_type=f32
-        ).astype(bf16)
-
-        @pl.when(d != 0)
-        def _():
-            rs_copy(d).start()
+            normed.append((gated * scale * gain_ref[:, cols]).astype(bf16))
+        out = jnp.dot(jnp.concatenate(normed, axis=1), wout_scr[...], preferred_element_type=f32).astype(bf16)
+        part_scr[d, 0] = out[:, :half]
+        part_scr[d, 1] = out[:, half:]
+
+        @pl.when(i == 0)
+        def _():
+            rs_copy(0).start()
+            rs_copy(1).start()
+
+        @pl.when(i == 1)
+        def _():
+            rs_copy(3).start()
+
+        @pl.when(i == 2)
+        def _():
+            rs_copy(4).start()
 
         return carry
 
     lax.fori_loop(0, n_tp, mix_rows, 0)
-    mixed = part_scr[0].astype(f32)
-    for d in (1, 3, 2):
-        rs_copy(d).wait_recv()
-        mixed = mixed + rs_in[d].astype(f32)
+    for k, d in ((0, 1), (1, 3)):
+        rs_copy(k).wait_recv()
+        part_scr[d, k] = (part_scr[d, k].astype(f32) + relay[k].astype(f32)).astype(bf16)
+        rs_copy((2, 5)[k]).start()
+    send_weight(2)
+    mixed = [part_scr[0, h].astype(f32) for h in range(2)]
+    for k in (3, 4, 2, 5):
+        rs_copy(k).wait_recv()
+        mixed[k % 2] = mixed[k % 2] + rs_in[(k - 2) // 2, k % 2].astype(f32)
+    mixed = jnp.concatenate(mixed, axis=1)
     middle = norm_rows(ALPHA * res_scr[...].astype(f32) + mixed, g1_ref[...], b1_ref[...]).astype(bf16).astype(f32)
     for c in range(chunks):
         tmpf[pl.ds(c, rows_here, stride=chunks), :] = middle[:, c * LANES : (c + 1) * LANES]
     mid3[...] = tmpf[0 : rows_here * chunks, :].reshape(rows_here, chunks, LANES).astype(bf16)
 
-    def send_plane(i, carry):
-        zt = lax.rem(z + plane_of(i), PLANES)
-
-        def send_one(j, carry):
-            t = zt * Y_CORES + lax.rem(yc + j, Y_CORES)
-            for k in range(CAP):
-                out5[t, k] = mid3[src_ref[t * CAP + k]]
-            same = lax.rem(t, 2) == odd
-            slot = (i * 2 + jnp.where(same, 0, 1)) * Y_CORES + yc
-            mine = jnp.logical_and(t == s, same)
-
-            @pl.when(mine)
+    def fill(t):
+        for k in range(CAP):
+            out5[t, k] = mid3[src_ref[t * CAP + k]]
+
+    stay = jnp.where(is_root, 0, 1)
+
+    def send_plane(i, away):
+        plane = lax.rem(z + SHIFTS[i], PLANES)
+        for m in range(Y_CORES // 2):
+            t = plane * Y_CORES + lax.rem(yc + 2 * m + (1 - stay if away else stay), Y_CORES)
+            slot = (i * 2 + away) * Y_CORES + yc
+            fill(t)
+
+            def send():
+                remote(
+                    out5.at[t], rin.at[slot], d_s.at[PLANES if away else i], d_r.at[i // 2],
+                    (t, beyond(plane) if away else x),
+                ).start()
+
+            if SHIFTS[i] == 0 and m == 0 and not away:
+
+                @pl.when(is_root)
+                def _():
+                    rin[slot] = out5[s]
+
+                pl.when(jnp.logical_not(is_root))(send)
+            else:
+                send()
+
+    def sent_plane(i):
+        def wait(count):
+            got(out5.at[pl.ds(0, count)], d_s.at[i], d_r.at[0]).wait_send()
+
+        if i < PLANES and SHIFTS[i] == 0:
+
+            @pl.when(is_root)
             def _():
-                rin[slot] = out5[t]
-
-            @pl.when(jnp.logical_not(mine))
+                wait(Y_CORES // 2 - 1)
+
+            @pl.when(jnp.logical_not(is_root))
             def _():
-                remote(out5.at[t], rin.at[slot], d_s, d_r.at[i // 2], (t, jnp.where(same, x, xp))).start()
-
-            return carry
-
-        lax.fori_loop(0, Y_CORES, send_one, 0)
-        return carry
-
-    lax.fori_loop(0, PLANES, send_plane, 0)
-
+                wait(Y_CORES // 2)
+
+        else:
+            wait(Y_CORES // 2 if i < PLANES else n_sp // 2)
+
+    def next_weight(k):
+        @pl.when(is_root)
+        def _():
+            sent_weight(k - 2, True)
+
+        @pl.when(jnp.logical_not(is_root))
+        def _():
+            sent_weight(k - 2, False)
+
+        send_weight(k)
+
+    for i in range(PLANES):
+        send_plane(i, 1)
+    send_weight(3)
+    send_weight(4)
+    send_plane(0, 0)
+    send_plane(1, 0)
+    for i in range(2, PLANES):
+        sent_plane(i - 2)
+        send_plane(i, 0)
+        if i == 5:
+            next_weight(5)
+    next_weight(6)
     quarter = 4 * Y_CORES
+    n = quarter * CAP
+    senders = 2 * n_sp
+    own_plane = SHIFTS.index(0)
+    own_chunk = own_plane // 2
+
+    def landed(m, first, count, sem):
+        ref = wbuf.at[m, pl.ds(0, n_tp - 1), pl.ds(first, count)]
+        remote(ref, ref, w_s.at[0], w_r.at[sem], (lax.rem(s + 1, n_sp), x)).wait_recv()
 
     @pl.when(is_root)
     def _():
-        for m in range(3):
-            pltpu.make_async_copy(experts_w[m].at[0], wbuf.at[m, x], wlsem.at[m]).wait()
-            ref = wbuf.at[m, pl.ds(0, n_tp - 1)]
-            remote(ref, ref, w_s.at[m, 0], w_r.at[m], (lax.rem(s + 1, n_sp), x)).wait_recv()
+        own_weight(0).wait()
+        landed(0, 0, model, 0)
 
         def expert_chunk(ci, carry):
             base = ci * quarter
 
-            @pl.when(ci < 3)
+            @pl.when(ci != own_chunk)
             def _():
-                got(rin.at[pl.ds(0, quarter)], d_s, d_r.at[ci]).wait_recv()
-
-            @pl.when(ci == 3)
+                got(rin.at[pl.ds(0, quarter)], d_s.at[0], d_r.at[ci]).wait_recv()
+
+            @pl.when(ci == own_chunk)
             def _():
-                got(rin.at[pl.ds(0, quarter - 1)], d_s, d_r.at[ci]).wait_recv()
-
-            n = quarter * CAP
-            tmpf[...] = rin[pl.ds(base, quarter)].astype(f32).reshape(n * chunks, LANES)
+                got(rin.at[pl.ds(0, quarter - 1)], d_s.at[0], d_r.at[ci]).wait_recv()
+
+            tmpf[0 : n * chunks, :] = rin[pl.ds(base, quarter)].astype(f32).reshape(n * chunks, LANES)
+            rows = pl.ds(pl.multiple_of(ci * n, n), n)
             for c in range(chunks):
-                xrow[:, c * LANES : (c + 1) * LANES] = tmpf[pl.ds(c, n, stride=chunks), :].astype(bf16)
+                xrow[rows, c * LANES : (c + 1) * LANES] = tmpf[pl.ds(c, n, stride=chunks), :].astype(bf16)
             for t in range(n_tp):
-                gate = jnp.dot(xrow[...], wbuf[0, t], preferred_element_type=f32)
-                up = jnp.dot(xrow[...], wbuf[1, t], preferred_element_type=f32)
-                hid[t] = (silu(gate) * up).astype(bf16)
-            for o in range(chunks // 2):
+                gated_scr[t, rows, :] = jnp.dot(xrow[rows, :], wbuf[0, t], preferred_element_type=f32)
+            return carry
+
+        lax.fori_loop(0, 4, expert_chunk, 0)
+        own_weight(1).wait()
+        landed(1, 0, model, 1)
+
+        def expert_up(t, carry):
+            up = jnp.dot(xrow[...], wbuf[1, t], preferred_element_type=f32)
+            hid[t] = (silu(gated_scr[t]) * up).astype(bf16)
+            return carry
+
+        lax.fori_loop(0, n_tp, expert_up, 0)
+        next_weight(7)
+        next_weight(8)
+        own_weight(2).wait()
+
+        fourth = chunks // 4
+
+        def answer_part(h, carry):
+            landed(2, h * piece, piece, 2 + h)
+            for o in range(fourth // 2):
                 ans = None
                 for t in range(n_tp):
                     part = lax.dot_general(
-                        hid[t], wbuf[2, t, 2 * o * LANES : 2 * (o + 1) * LANES, :],
+                        hid[t], wbuf[2, t, pl.ds(pl.multiple_of(h * piece + 2 * o * LANES, 2 * LANES), 2 * LANES), :],
                         (((1,), (1,)), ((), ())), preferred_element_type=f32,
                     )
                     ans = part if ans is None else ans + part
-                tmpf[pl.ds(2 * o, n, stride=chunks), :] = ans[:, :LANES]
-                tmpf[pl.ds(2 * o + 1, n, stride=chunks), :] = ans[:, LANES:]
-            ansb[pl.ds(base, quarter)] = tmpf[...].reshape(quarter, CAP, chunks, LANES).astype(bf16)
-
-            def send_back(m, carry):
-                slot = base + m
-                i = slot // 16
-                same = lax.rem(slot // 8, 2) == 0
-                t = lax.rem(z + PLANES - plane_of(i), PLANES) * Y_CORES + lax.rem(slot, 8)
-                mine = jnp.logical_and(t == s, same)
-
-                @pl.when(mine)
-                def _():
-                    fin[s] = ansb[slot]
-
-                @pl.when(jnp.logical_not(mine))
-                def _():
-                    remote(ansb.at[slot], fin.at[s], f_s, f_r, (t, jnp.where(same, x, xp))).start()
-
-                return carry
-
-            lax.fori_loop(0, quarter, send_back, 0)
+                tmpf[pl.ds(2 * o, senders * CAP, stride=fourth), :] = ans[:, :LANES]
+                tmpf[pl.ds(2 * o + 1, senders * CAP, stride=fourth), :] = ans[:, LANES:]
+            ansb[h] = tmpf[0 : senders * CAP * fourth, :].reshape(senders, CAP, fourth, LANES).astype(bf16)
+
+            for i in range(PLANES):
+                base = lax.rem(z + PLANES - SHIFTS[i], PLANES) * Y_CORES
+                for g in range(2):
+                    for j in range(1 if i == own_plane and g == 0 else 0, Y_CORES):
+                        y = lax.rem(yc + j, Y_CORES)
+                        slot = (i * 2 + g) * Y_CORES + y
+                        remote(
+                            ansb.at[h, slot], fin.at[h, s], f_s, f_r.at[h], (base + y, x if g == 0 else xp)
+                        ).start()
+            fin[h, s] = ansb[h, own_plane * 2 * Y_CORES + yc]
             return carry
 
-        lax.fori_loop(0, 4, expert_chunk, 0)
-        got(fin.at[pl.ds(0, n_sp - 1)], f_s, f_r).wait_recv()
+        lax.fori_loop(0, 4, answer_part, 0)
 
     @pl.when(jnp.logical_not(is_root))
     def _():
-        got(fin.at[pl.ds(0, n_sp)], f_s, f_r).wait_recv()
-
-    def combine(r, carry):
-        total = ALPHA * mid3[r].astype(f32)
-        ffn = None
-        for k in range(2):
-            slot = slot_ref[2 * r + k]
-            part = fin[slot // CAP, lax.rem(slot, CAP)].astype(f32) * rw_ref[2 * r + k]
-            ffn = part if ffn is None else ffn + part
-        tmpf[pl.ds(pl.multiple_of(r * chunks, chunks), chunks), :] = total + ffn
-        return carry
-
-    lax.fori_loop(0, rows_here, combine, 0, unroll=4)
+        next_weight(7)
+        next_weight(8)
+
+    fourth = chunks // 4
+    for h in range(4):
+
+        @pl.when(is_root)
+        def _():
+            got(fin.at[h, pl.ds(0, n_sp - 1)], f_s, f_r.at[h]).wait_recv()
+
+        @pl.when(jnp.logical_not(is_root))
+        def _():
+            got(fin.at[h], f_s, f_r.at[h]).wait_recv()
+
+        def combine(r, carry):
+            total = ALPHA * mid3[r, h * fourth : (h + 1) * fourth].astype(f32)
+            ffn = None
+            for k in range(2):
+                slot = slot_ref[k * rows_here + r]
+                one = stage[slot // CAP, lax.rem(slot, CAP)].astype(f32) * rw_ref[k, r]
+                ffn = one if ffn is None else ffn + one
+            tmpf[pl.ds(pl.multiple_of(r * chunks + h * fourth, fourth), fourth), :] = total + ffn
+            return carry
+
+        stage[...] = fin[h]
+        lax.fori_loop(0, rows_here, combine, 0, unroll=8)
     total = jnp.concatenate([tmpf[pl.ds(c, rows_here, stride=chunks), :] for c in range(chunks)], axis=1)
     o_ref[...] = norm_rows(total, g2_ref[...], b2_ref[...]).astype(bf16)
 
@@ -454,33 +583,32 @@
     got(logs_in.at[pl.ds(0, n_sp - 1)], log_s, log_r).wait_send()
     got(xin.at[pl.ds(0, n_sp - 1)], ex_s, ex_r).wait_send()
     got(ein.at[pl.ds(0, n_sp - 1)], en_s, en_r).wait_send()
-    for d in range(1, n_tp):
-        rs_copy(d).wait_send()
+    for k in range(6):
+        rs_copy(k).wait_send()
+    for i in range(PLANES - 2, PLANES + 1):
+        sent_plane(i)
 
     @pl.when(is_root)
     def _():
-        for m in range(3):
-            weight_copy(m, 0, lax.rem(x + 2, n_tp)).wait_send()
-        got(out5.at[pl.ds(0, n_sp - 1)], d_s, d_r.at[0]).wait_send()
-        got(ansb.at[pl.ds(0, 2 * n_sp - 1)], f_s, f_r).wait_send()
+        for k in (0, 1, 2, 7, 8):
+            sent_weight(k, True)
+        got(ansb.at[pl.ds(0, 4), pl.ds(0, senders - 1)], f_s, f_r.at[0]).wait_send()
 
     @pl.when(jnp.logical_not(is_root))
     def _():
-        for m in range(3):
-            weight_copy(m, 0, lax.rem(x + 1, n_tp)).wait_send()
-            weight_copy(m, 1, lax.rem(x + 3, n_tp)).wait_send()
-        got(out5.at[pl.ds(0, n_sp)], d_s, d_r.at[0]).wait_send()
-
-
-def slot_layout(block_routes, capacity, experts):
-    flat_routes = block_routes.reshape(-1)
-    n = flat_routes.shape[0]
-    earlier = jnp.arange(n)[:, None] > jnp.arange(n)[None, :]
-    same = flat_routes[:, None] == flat_routes[None, :]
-    rank = jnp.sum((earlier & same).astype(jnp.int32), axis=1)
-    slots = flat_routes * capacity + rank
-    hit = slots[:, None] == jnp.arange(experts * capacity, dtype=jnp.int32)[None, :]
-    source = jnp.sum(jnp.where(hit, (jnp.arange(n, dtype=jnp.int32) // block_routes.shape[1])[:, None], 0), axis=0)
+        for k in (0, 1, 2, 7, 8):
+            sent_weight(k, False)
+
+
+def slot_layout(by_rank):
+    top, rows = by_rank.shape
+    flat = by_rank.reshape(-1)
+    row = jnp.arange(top * rows, dtype=jnp.int32) % rows
+    earlier = row[:, None] > row[None, :]
+    rank = jnp.sum((earlier & (flat[:, None] == flat[None, :])).astype(jnp.int32), axis=1)
+    slots = flat * CAP + rank
+    hit = slots[:, None] == jnp.arange(N_EXPERTS * CAP, dtype=jnp.int32)[None, :]
+    source = jnp.sum(jnp.where(hit, row[:, None], 0), axis=0)
     return slots, source
 
 
@@ -500,9 +628,9 @@
     hidden = expert_gate_weight.shape[2]
     chunks = model // LANES
     panels = width // LANES
-    slots, source = slot_layout(routes, CAP, n_sp)
+    slots, source = slot_layout(routes.T)
     dma = pltpu.SemaphoreType.DMA
-    quarter_rows = 4 * Y_CORES * CAP
+    root_rows = 2 * n_sp * CAP
     return pl.pallas_call(
         layer_kernel,
         out_shape=jax.ShapeDtypeStruct((rows_here, model), bf16),
@@ -532,19 +660,22 @@
             pltpu.VMEM((n_sp, 16, LANES), bf16),
             pltpu.VMEM((n_sp, 16, LANES), bf16),
             pltpu.VMEM((n_sp, 16, LANES), bf16),
-            pltpu.VMEM((n_tp, rows_here, model), bf16),
-            pltpu.VMEM((n_tp, rows_here, model), bf16),
+            pltpu.VMEM((n_tp, 2, rows_here, model // 2), bf16),
+            pltpu.VMEM((2, rows_here, model // 2), bf16),
+            pltpu.VMEM((2, 2, rows_here, model // 2), bf16),
             pltpu.VMEM((rows_here, chunks, LANES), bf16),
-            pltpu.VMEM((quarter_rows * chunks, LANES), f32),
+            pltpu.VMEM((root_rows * chunks // 2, LANES), f32),
             pltpu.VMEM((n_sp, CAP, chunks, LANES), bf16),
             pltpu.VMEM((2 * n_sp, CAP, chunks, LANES), bf16),
-            pltpu.VMEM((quarter_rows, model), bf16),
-            pltpu.VMEM((n_tp, quarter_rows, hidden), bf16),
-            pltpu.VMEM((2 * n_sp, CAP, chunks, LANES), bf16),
-            pltpu.VMEM((n_sp, CAP, chunks, LANES), bf16),
+            pltpu.VMEM((root_rows, model), bf16),
+            pltpu.VMEM((n_tp, root_rows, hidden), f32),
+            pltpu.VMEM((n_tp, root_rows, hidden), bf16),
+            pltpu.VMEM((4, 2 * n_sp, CAP, chunks // 4, LANES), bf16),
+            pltpu.VMEM((4, n_sp, CAP, chunks // 4, LANES), bf16),
+            pltpu.VMEM((n_sp, CAP, chunks // 4, LANES), bf16),
             pltpu.VMEM((3, n_tp, model, hidden), bf16),
             dma((6,)), dma((3,)), dma((3,)), dma((3,)), dma, dma, dma, dma, dma, dma,
-            dma((n_tp,)), dma((n_tp,)), dma((3, 2)), dma((3,)), dma, dma((4,)), dma, dma,
+            dma((6,)), dma((6,)), dma((9,)), dma((6,)), dma((PLANES + 1,)), dma((4,)), dma, dma((4,)),
         ],
         compiler_params=pltpu.CompilerParams(
             collective_id=0, has_side_effects=True, vmem_limit_bytes=60 * 1024 * 1024
@@ -552,11 +683,11 @@
         name="layer",
     )(
         head_input_values, group_input_vectors, group_readout_vectors, output_gate_values,
-        step_size_logits, extra_log_decay, head_input_filter, input_vector_filter, readout_vector_filter,
+        step_size_logits.T, extra_log_decay.T, head_input_filter, input_vector_filter, readout_vector_filter,
         step_size_bias.reshape(1, heads), head_rate_logarithm.reshape(1, heads), direct_path_weight.reshape(1, heads),
-        group_norm_scale.reshape(1, width), mixer_output_weight, residual,
+        group_norm_scale.astype(f32).reshape(1, width), mixer_output_weight, residual,
         first_norm_scale.reshape(1, model), first_norm_bias.reshape(1, model),
-        source, slots, routing_weight.reshape(-1),
+        source, slots, routing_weight.T,
         expert_gate_weight, expert_up_weight, expert_down_weight,
         final_norm_scale.reshape(1, model), final_norm_bias.reshape(1, model),
     )

time: 176 us -> 140 us (0.80)
  Pallas kernels: 165 us -> 135 us
  local copies, waits for them, and re-layouts: 8.55 us -> 2.53 us
    pallas_call x1, Pallas kernels: 165 us -> 135 us  [shards(): pl.pallas_call(layer_kernel, out_shape=jax.ShapeDtypeStruct((rows_here, m...]
    unnamed x7 -> x3, local copies, waits for them, and re-layouts: 6.41 us -> 1.77 us
where the time goes in v2:
time: 140 us
  Pallas kernels  135 us (96%)
  local copies, waits for them, and re-layouts  2.53 us (2%)
  other arithmetic  2.21 us (2%)
    pallas_call x1, Pallas kernels, shards(): pl.pallas_call(layer_kernel, out_shape=jax.ShapeDtypeStruct((rows_here, m...  135 us

profile of v2, /device:TPU:1, one launch (start us, length us, event | category | flops | bytes accessed | tf_op | source)
XLA Modules:
  0.0 139.9 jit_solution(1037400661326361062)
XLA Ops:
  0.0 0.8 reshape.64
  0.8 0.2 convert_reduce_fusion
  1.0 0.0 copy-start
  1.0 0.7 select_reduce_fusion.src_ref
  1.7 1.3 reshape.67
  3.0 0.0 copy-done
  3.0 135.1 %layer.1 = bf16[96,2048]{1,0:T(8,128)(2,1)} custom-call(bf16[384,1024]{1,0:T(8,128)(2,1)} %x_hbm.1, bf16[384,256]{1,0:T(8,128)(2,1)} %b_hbm.1, bf16[384,256]{1,0:T(8,128)(2,1)} %c_hbm.1, bf16[384,1024]{1,0:T(8,128)(2,1)} %gate_hbm.1, f32[16,384]{1,0:T(8,128)} %bitcast.12, f32[16,384]{1,0:T(8,128)} %bitcast.13, bf16[4,1024]{1,0:T(4,128)(2,1)} %fx_ref.1, ...), custom_call_target="tpu_custom_call" | custom-call | tf_op jit(solution)/shard_map/layer/pallas_call | solution.py:634
  138.1 1.8 %copy.26 = bf16[96,2048]{1,0:T(8,128)(2,1)} copy(bf16[96,2048]{1,0:T(8,128)(2,1)} %layer.1) | data formatting | bytes 786432
  (2 shorter events, 0.0 us)
Async XLA Ops:
  1.0 2.0 %copy-start = (s32[192]{0:T(256)}, s32[192]{0:T(256)S(1)}, u32[]{:S(2)}) copy-start(s32[192]{0:T(256)S(1)} %multiply_add_fusion.slot_ref) | copy-start | bytes 2308

commit v3 on v2

--- a/solution.py
+++ b/solution.py
@@ -14,7 +14,6 @@
 ALPHA = 8.0**0.25
 LANES = 128
 CAP = 5
-N_EXPERTS = 64
 Y_CORES = 8
 PLANES = 8
 
@@ -50,12 +49,12 @@
 def layer_kernel(
     x_hbm, b_hbm, c_hbm, gate_hbm, logit_ref, extra_ref, fx_ref, fb_ref, fc_ref,
     bias_ref, rate_ref, direct_ref, gain_ref, wout_hbm, res_hbm, g1_ref, b1_ref,
-    src_ref, slot_ref, rw_ref, wg_hbm, wu_hbm, wd_hbm, g2_ref, b2_ref,
+    route_ref, rw_ref, wg_hbm, wu_hbm, wd_hbm, g2_ref, b2_ref,
     o_ref,
     x_scr, b_scr, c_scr, gate_scr, wout_scr, res_scr,
     tailx, tailb, tailc, pad_scr, y_scr, u_scr, bb_scr, cc_scr, run_scr, st_scr, gs_scr,
     logs_out, logs_in, pack, xin, eout, ein,
-    part_scr, relay, rs_in, mid3, tmpf, out5, rin, xrow, gated_scr, hid, ansb, fin, stage, wbuf,
+    part_scr, relay, rs_in, mid3, tmpf, out5, rin, xrow, gated_scr, hid, ansb, fin, stage, wbuf, table, src_ref, slot_ref,
     lsem, wlsem, tail_s, tail_r, log_s, log_r, ex_s, ex_r, en_s, en_r, rs_s, rs_r, w_s, w_r, d_s, d_r, f_s, f_r,
 ):
     n_sp, n_tp = 64, 4
@@ -181,6 +180,25 @@
         before = before + r[L - 1 : L]
     for p in range(panels):
         logs_out[p] = pair_wide(before, p)
+    experts = n_sp
+    name = lax.broadcasted_iota(jnp.int32, (experts, rows_here), 0)
+    named = [(name == route_ref[k : k + 1, :]).astype(f32) for k in range(2)]
+    both = named[0] + named[1]
+    ri = lax.broadcasted_iota(jnp.int32, (rows_here, rows_here), 0)
+    rj = lax.broadcasted_iota(jnp.int32, (rows_here, rows_here), 1)
+    earlier = jnp.dot(both.astype(bf16), (ri < rj).astype(bf16), preferred_element_type=f32)
+    for k in range(2):
+        rank = jnp.sum(named[k] * earlier, axis=0, keepdims=True)
+        table[1, k : k + 1, 0:rows_here] = route_ref[k : k + 1, :] * CAP + rank.astype(jnp.int32)
+    both_t, earlier_t = both.T, earlier.T
+    token = lax.broadcasted_iota(jnp.int32, (rows_here, experts), 0).astype(f32)
+    for k in range(CAP):
+        here_k = jnp.logical_and(both_t > 0.5, jnp.abs(earlier_t - k) < 0.5)
+        table[0, k : k + 1, 0:experts] = jnp.sum(jnp.where(here_k, token, 0.0), axis=0, keepdims=True).astype(jnp.int32)
+    tables = [
+        pltpu.make_async_copy(table.at[0], src_ref, lsem.at[6]),
+        pltpu.make_async_copy(table.at[1], slot_ref, lsem.at[7]),
+    ]
     here[3].wait()
 
     def gate_rows(i, carry):
@@ -191,6 +209,8 @@
     lax.fori_loop(0, length // 32, gate_rows, 0)
     for copy in here[:3]:
         copy.wait()
+    for copy in tables:
+        copy.start()
 
     pl.semaphore_wait(barrier, n_sp - 1 + n_tp - 1 + n_sp // 2 + jnp.where(is_root, n_sp, 0))
 
@@ -397,9 +417,11 @@
         tmpf[pl.ds(c, rows_here, stride=chunks), :] = middle[:, c * LANES : (c + 1) * LANES]
     mid3[...] = tmpf[0 : rows_here * chunks, :].reshape(rows_here, chunks, LANES).astype(bf16)
 
+    for copy in tables:
+        copy.wait()
     def fill(t):
         for k in range(CAP):
-            out5[t, k] = mid3[src_ref[t * CAP + k]]
+            out5[t, k] = mid3[jnp.clip(src_ref[k, t], 0, rows_here - 1)]
 
     stay = jnp.where(is_root, 0, 1)
 
@@ -501,6 +523,7 @@
             return carry
 
         lax.fori_loop(0, 4, expert_chunk, 0)
+        next_weight(7)
         own_weight(1).wait()
         landed(1, 0, model, 1)
 
@@ -510,8 +533,6 @@
             return carry
 
         lax.fori_loop(0, n_tp, expert_up, 0)
-        next_weight(7)
-        next_weight(8)
         own_weight(2).wait()
 
         fourth = chunks // 4
@@ -540,6 +561,11 @@
                             ansb.at[h, slot], fin.at[h, s], f_s, f_r.at[h], (base + y, x if g == 0 else xp)
                         ).start()
             fin[h, s] = ansb[h, own_plane * 2 * Y_CORES + yc]
+
+            @pl.when(h == 0)
+            def _():
+                next_weight(8)
+
             return carry
 
         lax.fori_loop(0, 4, answer_part, 0)
@@ -564,7 +590,7 @@
             total = ALPHA * mid3[r, h * fourth : (h + 1) * fourth].astype(f32)
             ffn = None
             for k in range(2):
-                slot = slot_ref[k * rows_here + r]
+                slot = jnp.clip(slot_ref[k, r], 0, n_sp * CAP - 1)
                 one = stage[slot // CAP, lax.rem(slot, CAP)].astype(f32) * rw_ref[k, r]
                 ffn = one if ffn is None else ffn + one
             tmpf[pl.ds(pl.multiple_of(r * chunks + h * fourth, fourth), fourth), :] = total + ffn
@@ -598,18 +624,6 @@
     def _():
         for k in (0, 1, 2, 7, 8):
             sent_weight(k, False)
-
-
-def slot_layout(by_rank):
-    top, rows = by_rank.shape
-    flat = by_rank.reshape(-1)
-    row = jnp.arange(top * rows, dtype=jnp.int32) % rows
-    earlier = row[:, None] > row[None, :]
-    rank = jnp.sum((earlier & (flat[:, None] == flat[None, :])).astype(jnp.int32), axis=1)
-    slots = flat * CAP + rank
-    hit = slots[:, None] == jnp.arange(N_EXPERTS * CAP, dtype=jnp.int32)[None, :]
-    source = jnp.sum(jnp.where(hit, row[:, None], 0), axis=0)
-    return slots, source
 
 
 def shards(
@@ -628,13 +642,12 @@
     hidden = expert_gate_weight.shape[2]
     chunks = model // LANES
     panels = width // LANES
-    slots, source = slot_layout(routes.T)
     dma = pltpu.SemaphoreType.DMA
     root_rows = 2 * n_sp * CAP
     return pl.pallas_call(
         layer_kernel,
         out_shape=jax.ShapeDtypeStruct((rows_here, model), bf16),
-        in_specs=[HBM] * 4 + [VMEM] * 9 + [HBM] * 2 + [VMEM] * 2 + [SMEM] * 3 + [HBM] * 3 + [VMEM] * 2,
+        in_specs=[HBM] * 4 + [VMEM] * 9 + [HBM] * 2 + [VMEM] * 3 + [SMEM] + [HBM] * 3 + [VMEM] * 2,
         out_specs=VMEM,
         scratch_shapes=[
             pltpu.VMEM((length, width), bf16),
@@ -674,7 +687,10 @@
             pltpu.VMEM((4, n_sp, CAP, chunks // 4, LANES), bf16),
             pltpu.VMEM((n_sp, CAP, chunks // 4, LANES), bf16),
             pltpu.VMEM((3, n_tp, model, hidden), bf16),
-            dma((6,)), dma((3,)), dma((3,)), dma((3,)), dma, dma, dma, dma, dma, dma,
+            pltpu.VMEM((2, 8, LANES), jnp.int32),
+            pltpu.SMEM((8, LANES), jnp.int32),
+            pltpu.SMEM((8, LANES), jnp.int32),
+            dma((8,)), dma((3,)), dma((3,)), dma((3,)), dma, dma, dma, dma, dma, dma,
             dma((6,)), dma((6,)), dma((9,)), dma((6,)), dma((PLANES + 1,)), dma((4,)), dma, dma((4,)),
         ],
         compiler_params=pltpu.CompilerParams(
@@ -687,7 +703,7 @@
         step_size_bias.reshape(1, heads), head_rate_logarithm.reshape(1, heads), direct_path_weight.reshape(1, heads),
         group_norm_scale.astype(f32).reshape(1, width), mixer_output_weight, residual,
         first_norm_scale.reshape(1, model), first_norm_bias.reshape(1, model),
-        source, slots, routing_weight.T,
+        routes.T, routing_weight.T,
         expert_gate_weight, expert_up_weight, expert_down_weight,
         final_norm_scale.reshape(1, model), final_norm_bias.reshape(1, model),
     )

time: 140 us -> 138 us (0.986)
  no operation moved by 1% of the time
where the time goes in v3:
time: 138 us
  Pallas kernels  134 us (97%)
  local copies, waits for them, and re-layouts  1.77 us (1%)
    pallas_call x1, Pallas kernels, shards(): pl.pallas_call(layer_kernel, out_shape=jax.ShapeDtypeStruct((rows_here, m...  134 us

profile of v3, /device:TPU:1, one launch (start us, length us, event | category | flops | bytes accessed | tf_op | source)
XLA Modules:
  0.0 137.5 jit_solution(11187705587725634276)
XLA Ops:
  0.0 1.3 reshape.35
  1.3 134.5 %layer.1 = bf16[96,2048]{1,0:T(8,128)(2,1)} custom-call(bf16[384,1024]{1,0:T(8,128)(2,1)} %x_hbm.1, bf16[384,256]{1,0:T(8,128)(2,1)} %b_hbm.1, bf16[384,256]{1,0:T(8,128)(2,1)} %c_hbm.1, bf16[384,1024]{1,0:T(8,128)(2,1)} %gate_hbm.1, f32[16,384]{1,0:T(8,128)} %bitcast.12, f32[16,384]{1,0:T(8,128)} %bitcast.13, bf16[4,1024]{1,0:T(4,128)(2,1)} %fx_ref.1, ...), custom_call_target="tpu_custom_call" | custom-call | tf_op jit(solution)/shard_map/layer/pallas_call | solution.py:647
  135.8 1.8 %copy.26 = bf16[96,2048]{1,0:T(8,128)(2,1)} copy(bf16[96,2048]{1,0:T(8,128)(2,1)} %layer.1) | data formatting | bytes 786432
